TPU v7x, 512 devices: a whole 4x4x16 slice. The times are simulated.
512 devices in a mesh: ep: 32 (over z, core), tp: 16 (over y, x).
Axes of the slice: x: 4, y: 4, z: 16, core: 2. Of those that a mesh axis runs over, the one named last changes fastest.
Arguments:
- mixer_input: bfloat16 [4096, 2048], P('ep'), may hold values from -6 to 6
- mixer_gain: float32 [2048], replicated, may hold values from 0.1 to 1.9
- glu_value_weight: bfloat16 [512, 2048], P('tp'), may hold values from -0.125 to 0.125
- glu_gate_weight: bfloat16 [512, 2048], P('tp'), may hold values from -0.125 to 0.125
- conv_taps: float32 [512, 31], P('tp'), may hold values from -1 to 1
- conv_bias: float32 [512], P('tp'), may hold values from -3 to 3
- channel_gain: float32 [512], replicated, may hold values from 0.1 to 1.9
- channel_shift: float32 [512], replicated, may hold values from -3 to 3
- mixer_out_weight: bfloat16 [512, 2048], P(None, 'tp'), may hold values from -0.25 to 0.25
- expert_input: bfloat16 [8192, 2048], P('ep'), may hold values from -6 to 6
- expert_gain: float32 [2048], replicated, may hold values from 0.1 to 1.9
- routes: int32 [8192, 2], P('ep'), may hold values from 0 to 31, all different within a row; in each aligned block of 256 rows (0 to 255, 256 to 511, ...) at most 24 rows name the same one
- route_logits: float32 [8192, 2], P('ep'), may hold values from -8 to 8
- gate_weight: bfloat16 [32, 2048, 4096], P('ep', None, 'tp'), may hold values from -0.125 to 0.125
- up_weight: bfloat16 [32, 2048, 4096], P('ep', None, 'tp'), may hold values from -0.125 to 0.125
- down_weight: bfloat16 [32, 4096, 2048], P('ep', 'tp'), may hold values from -0.09375 to 0.09375
Outputs:
- mixer_output: bfloat16 [4096, 2048], P('ep', 'tp')
- expert_output: bfloat16 [8192, 2048], P('ep', 'tp')
Inputs may be any that keep to these rules, and one draw needn't show every extreme that they name: `routes`: the 2 entries of a row differ. Among the rows of one index of ep, no expert is named by more than 24 rows, a bound that some block reaches.
All inputs are finite; a program needn't handle non-finite values.
Results may differ from a plain program's by a relative error of at most 0.015.
Values may be sent and summed in bfloat16 or wider, within the bound.
No kernel may reach another device: no remote copies, remote signals or barrier semaphores. Data moves between devices by JAX's collectives and lax.ppermute only.
A program may use at most 64 MiB of HBM per device.

v0:
```python
import jax
import jax.numpy as jnp
from jax import lax
from jax.sharding import PartitionSpec as P

norm_eps = 1e-06


def shifted(value, axis, steps):
    count = lax.axis_size(axis)
    first, last = (max(0, -steps), min(count, count - steps))
    return lax.ppermute(value, axis, [(source, source + steps) for source in range(first, last)])


def in_order(pieces, dim):
    dims = list(pieces.shape[1:])
    dims[dim] *= pieces.shape[0]
    return jnp.moveaxis(pieces, 0, dim).reshape(dims)


def from_everyone(shard, axis):
    copies = jnp.broadcast_to(shard, (lax.axis_size(axis), *shard.shape))
    return lax.all_to_all(copies, axis, split_axis=0, concat_axis=0, tiled=True)


def gathered_copies(shard, axis, dim):
    return in_order(from_everyone(shard, axis), dim)


def in_blocks(shard, dim, count):
    dims = shard.shape
    pieces = shard.reshape(*dims[:dim], count, dims[dim] // count, *dims[dim + 1 :])
    return jnp.moveaxis(pieces, dim, 0)


def sum_at_owner(shard, axis, dim):
    pieces = in_blocks(shard, dim, lax.axis_size(axis))
    arrived = lax.all_to_all(pieces, axis, split_axis=0, concat_axis=0, tiled=True)
    return arrived.astype(jnp.float32).sum(axis=0)


def rms_rows(row_block, gain_vec):
    row_values = row_block.astype(jnp.float32)
    inv_scale = lax.rsqrt(jnp.mean(row_values * row_values, axis=-1, keepdims=True) + norm_eps)
    return (row_values * inv_scale * gain_vec[None, :]).astype(jnp.bfloat16)


def on_device(
    mixer_input,
    mixer_gain,
    glu_value_weight,
    glu_gate_weight,
    conv_taps,
    conv_bias,
    channel_gain,
    channel_shift,
    mixer_out_weight,
    expert_input,
    expert_gain,
    routes,
    route_logits,
    gate_weight,
    up_weight,
    down_weight,
):
    normed_a = rms_rows(mixer_input, mixer_gain)
    contract = (((1,), (1,)), ((), ()))
    glu_value = lax.dot_general(
        glu_value_weight, normed_a, contract, preferred_element_type=jnp.float32
    )
    glu_gate = lax.dot_general(
        glu_gate_weight, normed_a, contract, preferred_element_type=jnp.float32
    )
    gated_rows = (glu_value * jax.nn.sigmoid(glu_gate)).astype(jnp.bfloat16)
    row_count = gated_rows.shape[1]
    reach_back = conv_taps.shape[1] - 1
    tail_rows = shifted(gated_rows[:, row_count - reach_back :], "ep", 1)
    padded = jnp.concatenate([tail_rows, gated_rows], axis=1).astype(jnp.float32)
    conv_sum = jnp.zeros(gated_rows.shape, jnp.float32)
    for offset in range(reach_back + 1):
        conv_sum = (
            conv_sum + conv_taps[:, offset : offset + 1] * padded[:, offset : offset + row_count]
        )
    conv_out = (conv_sum + conv_bias[:, None]).astype(jnp.bfloat16)
    all_channels = gathered_copies(conv_out, "tp", 0)
    chan_values = all_channels.astype(jnp.float32)
    chan_mean = jnp.mean(chan_values, axis=0, keepdims=True)
    centered = chan_values - chan_mean
    variance = jnp.mean(centered * centered, axis=0, keepdims=True)
    shaped = (
        centered * lax.rsqrt(variance + norm_eps) * channel_gain[:, None] + channel_shift[:, None]
    )
    activated = jax.nn.silu(shaped).astype(jnp.bfloat16)
    mixer_output = lax.dot_general(
        activated, mixer_out_weight, (((0,), (0,)), ((), ())), preferred_element_type=jnp.float32
    ).astype(jnp.bfloat16)
    normed_b = rms_rows(expert_input, expert_gain)
    rows_b = expert_input.shape[0]
    top_count = routes.shape[1]
    groups = lax.axis_size("ep")
    capacity = 3 * rows_b // groups
    assigned = routes.reshape(-1)
    matches = (assigned[:, None] == jnp.arange(groups, dtype=jnp.int32)[None, :]).astype(jnp.int32)
    earlier = jnp.cumsum(matches, axis=0) - matches
    slot_index = jnp.sum(earlier * matches, axis=1)
    slot_place = assigned * capacity + slot_index
    owner_row = jnp.arange(rows_b * top_count, dtype=jnp.int32) // top_count
    slot_owner = jnp.full((groups * capacity,), rows_b, jnp.int32).at[slot_place].set(owner_row)
    col_width = expert_input.shape[1] // lax.axis_size("tp")
    columns = lax.dynamic_slice_in_dim(normed_b, lax.axis_index("tp") * col_width, col_width, 1)
    outgoing = jnp.take(columns, slot_owner, axis=0, mode="fill", fill_value=0).reshape(
        groups, capacity, col_width
    )
    arrived = lax.all_to_all(outgoing, "ep", split_axis=0, concat_axis=0, tiled=True).reshape(
        groups * capacity, col_width
    )
    shard_piece = gathered_copies(arrived, "tp", 1)
    gate_rows = gate_weight[0]
    up_rows = up_weight[0]
    gate_acts = jnp.dot(shard_piece, gate_rows, preferred_element_type=jnp.float32)
    up_acts = jnp.dot(shard_piece, up_rows, preferred_element_type=jnp.float32)
    hidden = (jax.nn.silu(gate_acts) * up_acts).astype(jnp.bfloat16)
    partial_value = jnp.dot(hidden, down_weight[0], preferred_element_type=jnp.float32)
    summed = sum_at_owner(partial_value.astype(jnp.bfloat16), "tp", 1).astype(jnp.bfloat16)
    returned = lax.all_to_all(
        summed.reshape(groups, capacity, -1), "ep", split_axis=0, concat_axis=0, tiled=True
    ).reshape(groups * capacity, -1)
    picked = (
        jnp.take(returned, slot_place, axis=0).astype(jnp.float32).reshape(rows_b, top_count, -1)
    )
    first_weight = jax.nn.sigmoid(route_logits[:, 0] - route_logits[:, 1])
    second_weight = jax.nn.sigmoid(route_logits[:, 1] - route_logits[:, 0])
    combined = picked[:, 0] * first_weight[:, None] + picked[:, 1] * second_weight[:, None]
    return (mixer_output, combined.astype(jnp.bfloat16))


def solution(mesh):
    in_specs = (
        P("ep", None),
        P(),
        P("tp", None),
        P("tp", None),
        P("tp", None),
        P("tp"),
        P(),
        P(),
        P(None, "tp"),
        P("ep", None),
        P(),
        P("ep", None),
        P("ep", None),
        P("ep", None, "tp"),
        P("ep", None, "tp"),
        P("ep", "tp", None),
    )
    out_specs = (P("ep", "tp"), P("ep", "tp"))
    return jax.shard_map(
        on_device, mesh=mesh, in_specs=in_specs, out_specs=out_specs, check_vma=False
    )
```

profile of v0, /device:TPU:1, one launch (start us, length us, event | category | flops | bytes accessed | tf_op | source)
XLA Modules:
  0.0 206.3 jit_solution(10734175718234046916)
XLA Ops:
  0.7 1.6 convert_element_type.71
  2.3 0.3 multiply_reduce_fusion
  3.0 1.2 reduce-window.6
  4.2 0.2 slice_reduce_fusion
  4.9 2.4 %scatter_custom_fusion = s32[768]{0:T(1024)S(1)} fusion(s32[512]{0:T(512)S(1)} %bitcast.88, s32[512]{0:T(512)S(1)} %add_select_fusion, s32[]{:T(128)} %constant.78.clone.1), kind=kCustom, calls=%fused_computation.164 | custom fusion | bytes 3076 | tf_op jit(solution)/shard_map/scatter | solution.py:108
  7.5 0.8 dynamic-slice
  8.4 1.9 gather_fusion
  10.4 35.3 %all_to_all.25 = bf16[32,24,128]{2,1,0:T(8,128)(2,1)S(1)} all-to-all(bf16[32,24,128]{2,1,0:T(8,128)(2,1)S(1)} %broadcast_select_fusion), channel_id=1, replica_groups=mesh['ep'=32,'tp'=16] {'ep'}, dimensions={0} | all-to-all | bytes 393216 | tf_op jit(solution)/shard_map/all_to_all | solution.py:114
  45.9 2.0 broadcast_in_dim.53
  47.9 6.9 %all-to-all-start.2 = ((bf16[16,768,128]{1,2,0:T(8,128)(2,1)}), bf16[16,768,128]{1,2,0:T(8,128)(2,1)}, u32[]{:S(2)}, u32[]{:S(2)}) async-start(bf16[16,768,128]{1,2,0:T(8,128)(2,1)} %broadcast_in_dim.53), calls=%async_computation.2 | async-start | bytes 6291456 | tf_op jit(solution)/shard_map/all_to_all | solution.py:23
  54.9 0.2 fusion.8
  55.1 0.3 fusion.22
  55.5 0.4 fusion.7
  56.0 3.3 %collective-permute-start = (bf16[32,30]{1,0:T(8,128)(2,1)S(1)}, bf16[32,30]{1,0:T(8,128)(2,1)S(1)}, u32[]{:S(2)}, u32[]{:S(2)}) collective-permute-start(bf16[32,30]{1,0:T(8,128)(2,1)S(1)} %slice.282), channel_id=1, source_target_pairs={{0,16},{16,32},{32,48},{48,64},{64,80},{80,96},{96,112},{112,128},... | collective-permute-start | bytes 5768 | tf_op jit(solution)/shard_map/ppermute | solution.py:12
  59.3 0.5 slice_reduce_fusion.31
  59.9 0.4 slice_reduce_fusion.30
  60.4 0.3 fusion.37
  60.7 38.5 %all-to-all-done.2 = bf16[16,768,128]{1,2,0:T(8,128)(2,1)} async-done(((bf16[16,768,128]{1,2,0:T(8,128)(2,1)}), bf16[16,768,128]{1,2,0:T(8,128)(2,1)}, u32[]{:S(2)}, u32[]{:S(2)}) %all-to-all-start.2) | async-done | bytes 3145760 | tf_op jit(solution)/shard_map/all_to_all | solution.py:23
  99.2 0.7 broadcast_in_dim.46
  99.9 3.7 %all-to-all-start = ((bf16[16,32,128]{2,1,0:T(8,128)(2,1)}), bf16[16,32,128]{2,1,0:T(8,128)(2,1)S(1)}, u32[]{:S(2)}, u32[]{:S(2)}) async-start(bf16[16,32,128]{2,1,0:T(8,128)(2,1)} %broadcast_in_dim.46), calls=%async_computation | async-start | bytes 262144 | tf_op jit(solution)/shard_map/all_to_all | solution.py:23
  103.7 3.9 %fusion.13 = f32[768,256]{1,0:T(8,128)} fusion(bf16[768,2048]{0,1:T(8,128)(2,1)} %bitcast.8, bf16[1,2048,256]{2,1,0:T(8,128)(2,1)S(1)} %copy-done.10), kind=kOutput, calls=%fused_computation.24 | convolution fusion | flops 805306368 | bytes 4980736 | tf_op jit(solution)/shard_map/dot_general | solution.py:120
  107.6 7.1 %fusion = bf16[96,16,8,128]{3,2,1,0:T(8,128)(2,1)} fusion(bf16[1,256,2048]{2,1,0:T(8,128)(2,1)S(1)} %copy-done, bf16[768,2048]{0,1:T(8,128)(2,1)} %bitcast.8, bf16[1,2048,256]{2,1,0:T(8,128)(2,1)S(1)} %copy-done.11, f32[768,256]{1,0:T(8,128)} %fusion.13), kind=kOutput, calls=%fused_computation.6 | convolution fusion | flops 1613365248 | bytes 9175040 | tf_op jit(solution)/shard_map/dot_general | solution.py:123
  114.7 4.4 %copy.57 = bf16[96,16,8,128]{3,2,0,1:T(8,128)(2,1)} copy(bf16[96,16,8,128]{3,2,1,0:T(8,128)(2,1)} %fusion) | data formatting | bytes 6291456 | tf_op jit(solution)/shard_map/reshape | solution.py:32
  119.1 6.8 %all-to-all-start.3 = ((bf16[16,768,128]{2,1,0:T(8,128)(2,1)}), bf16[16,768,128]{2,1,0:T(8,128)(2,1)}, u32[]{:S(2)}, u32[]{:S(2)}) async-start(bf16[16,768,128]{2,1,0:T(8,128)(2,1)} %bitcast.82), calls=%async_computation.3 | async-start | bytes 6291456 | tf_op jit(solution)/shard_map/all_to_all | solution.py:38
  126.3 39.2 %all-to-all-done.3 = bf16[16,768,128]{2,1,0:T(8,128)(2,1)} async-done(((bf16[16,768,128]{2,1,0:T(8,128)(2,1)}), bf16[16,768,128]{2,1,0:T(8,128)(2,1)}, u32[]{:S(2)}, u32[]{:S(2)}) %all-to-all-start.3) | async-done | bytes 3145760 | tf_op jit(solution)/shard_map/all_to_all | solution.py:38
  165.5 3.0 %reduce_sum.68 = bf16[768,128]{1,0:T(8,128)(2,1)} reduce(bf16[16,768,128]{2,1,0:T(8,128)(2,1)} %all-to-all-done.3, bf16[]{:T(256)} %constant.85.clone.1), dimensions={0}, to_apply=%region_8.9 | reduce | flops 1474560 | bytes 3342338 | tf_op jit(solution)/shard_map/reduce_sum | solution.py:39
  168.6 16.7 %all-to-all-start.4 = ((bf16[32,24,128]{2,1,0:T(8,128)(2,1)}), bf16[32,24,128]{2,1,0:T(8,128)(2,1)S(1)}, u32[]{:S(2)}, u32[]{:S(2)}) async-start(bf16[32,24,128]{2,1,0:T(8,128)(2,1)} %bitcast.14), calls=%async_computation.4 | async-start | bytes 393216 | tf_op jit(solution)/shard_map/all_to_all | solution.py:125
  185.4 0.2 multiply_convert_fusion
  185.6 0.9 convolution_convert_fusion.1
  186.4 17.6 %all-to-all-done.4 = bf16[32,24,128]{2,1,0:T(8,128)(2,1)S(1)} async-done(((bf16[32,24,128]{2,1,0:T(8,128)(2,1)}), bf16[32,24,128]{2,1,0:T(8,128)(2,1)S(1)}, u32[]{:S(2)}, u32[]{:S(2)}) %all-to-all-start.4) | async-done | bytes 196640 | tf_op jit(solution)/shard_map/all_to_all | solution.py:125
  204.0 1.3 gather_fusion.1
  205.5 0.8 fusion.26
  (65 shorter events, 2.2 us)
Async XLA Ops:
  0.6 106.9 %copy-start = (bf16[1,256,2048]{2,1,0:T(8,128)(2,1)S(1)}, bf16[1,256,2048]{2,1,0:T(8,128)(2,1)}, u32[]{:S(2)}) copy-start(bf16[1,256,2048]{2,1,0:T(8,128)(2,1)} %param.31) | copy-start | bytes 3145732
  0.6 1.6 copy-start.2
  0.7 1.9 copy-start.5
  47.9 7.0 %copy-start.3 = (bf16[128,2048]{1,0:T(8,128)(2,1)S(1)}, bf16[128,2048]{1,0:T(8,128)(2,1)}, u32[]{:S(2)}) copy-start(bf16[128,2048]{1,0:T(8,128)(2,1)} %param.16) | copy-start | bytes 1572868
  47.9 7.2 %copy-start.12 = (bf16[32,2048]{1,0:T(8,128)(2,1)S(1)}, bf16[32,2048]{1,0:T(8,128)(2,1)}, u32[]{:S(2)}) copy-start(bf16[32,2048]{1,0:T(8,128)(2,1)} %param.18) | copy-start | bytes 393220
  47.9 7.2 %copy-start.14 = (f32[2048]{0:T(1024)S(1)}, f32[2048]{0:T(1024)}, u32[]{:S(2)}) copy-start(f32[2048]{0:T(1024)} %param.17) | copy-start | bytes 24580
  47.9 7.6 %copy-start.13 = (bf16[32,2048]{1,0:T(8,128)(2,1)S(1)}, bf16[32,2048]{1,0:T(8,128)(2,1)}, u32[]{:S(2)}) copy-start(bf16[32,2048]{1,0:T(8,128)(2,1)} %param.19) | copy-start | bytes 393220
  47.9 11.4 %copy-start.1 = (f32[32,31]{1,0:T(8,128)S(1)}, f32[32,31]{1,0:T(8,128)}, u32[]{:S(2)}) copy-start(f32[32,31]{1,0:T(8,128)} %param.20) | copy-start | bytes 11908
  47.9 51.3 %all-to-all-start.2 = ((bf16[16,768,128]{1,2,0:T(8,128)(2,1)}), bf16[16,768,128]{1,2,0:T(8,128)(2,1)}, u32[]{:S(2)}, u32[]{:S(2)}) async-start(bf16[16,768,128]{1,2,0:T(8,128)(2,1)} %broadcast_in_dim.53), calls=%async_computation.2 | async-start | bytes 6291456 | tf_op jit(solution)/shard_map/all_to_all | solution.py:23
  54.9 5.5 %copy-start.9 = (f32[32]{0:T(128)S(1)}, f32[32]{0:T(128)}, u32[]{:S(2)}) copy-start(f32[32]{0:T(128)} %param.21) | copy-start | bytes 388
  54.9 48.7 %copy-start.10 = (bf16[1,2048,256]{2,1,0:T(8,128)(2,1)S(1)}, bf16[1,2048,256]{2,1,0:T(8,128)(2,1)}, u32[]{:S(2)}) copy-start(bf16[1,2048,256]{2,1,0:T(8,128)(2,1)} %param.29) | copy-start | bytes 3145732
  56.0 4.3 %collective-permute-start = (bf16[32,30]{1,0:T(8,128)(2,1)S(1)}, bf16[32,30]{1,0:T(8,128)(2,1)S(1)}, u32[]{:S(2)}, u32[]{:S(2)}) collective-permute-start(bf16[32,30]{1,0:T(8,128)(2,1)S(1)} %slice.282), channel_id=1, source_target_pairs={{0,16},{16,32},{32,48},{48,64},{64,80},{80,96},{96,112},{112,128},... | collective-permute-start | bytes 5768 | tf_op jit(solution)/shard_map/ppermute | solution.py:12
  99.9 19.2 %all-to-all-start = ((bf16[16,32,128]{2,1,0:T(8,128)(2,1)}), bf16[16,32,128]{2,1,0:T(8,128)(2,1)S(1)}, u32[]{:S(2)}, u32[]{:S(2)}) async-start(bf16[16,32,128]{2,1,0:T(8,128)(2,1)} %broadcast_in_dim.46), calls=%async_computation | async-start | bytes 262144 | tf_op jit(solution)/shard_map/all_to_all | solution.py:23
  103.6 3.9 %copy-start.11 = (bf16[1,2048,256]{2,1,0:T(8,128)(2,1)S(1)}, bf16[1,2048,256]{2,1,0:T(8,128)(2,1)}, u32[]{:S(2)}) copy-start(bf16[1,2048,256]{2,1,0:T(8,128)(2,1)} %param.30) | copy-start | bytes 3145732
  119.1 7.1 %copy-start.8 = (f32[256,2]{0,1:T(2,128)S(1)}, f32[256,2]{0,1:T(2,128)}, u32[]{:S(2)}) copy-start(f32[256,2]{0,1:T(2,128)} %param.28) | copy-start | bytes 6148
  119.1 46.5 %all-to-all-start.3 = ((bf16[16,768,128]{2,1,0:T(8,128)(2,1)}), bf16[16,768,128]{2,1,0:T(8,128)(2,1)}, u32[]{:S(2)}, u32[]{:S(2)}) async-start(bf16[16,768,128]{2,1,0:T(8,128)(2,1)} %bitcast.82), calls=%async_computation.3 | async-start | bytes 6291456 | tf_op jit(solution)/shard_map/all_to_all | solution.py:38
  125.9 59.4 %copy-start.6 = (f32[512]{0:T(512)S(1)}, f32[512]{0:T(512)}, u32[]{:S(2)}) copy-start(f32[512]{0:T(512)} %param.23) | copy-start | bytes 6148
  125.9 59.4 %copy-start.7 = (f32[512]{0:T(512)S(1)}, f32[512]{0:T(512)}, u32[]{:S(2)}) copy-start(f32[512]{0:T(512)} %param.22) | copy-start | bytes 6148
  125.9 59.7 %copy-start.4 = (bf16[512,128]{1,0:T(8,128)(2,1)S(1)}, bf16[512,128]{1,0:T(8,128)(2,1)}, u32[]{:S(2)}) copy-start(bf16[512,128]{1,0:T(8,128)(2,1)} %param.24) | copy-start | bytes 393220
  168.6 35.5 %all-to-all-start.4 = ((bf16[32,24,128]{2,1,0:T(8,128)(2,1)}), bf16[32,24,128]{2,1,0:T(8,128)(2,1)S(1)}, u32[]{:S(2)}, u32[]{:S(2)}) async-start(bf16[32,24,128]{2,1,0:T(8,128)(2,1)} %bitcast.14), calls=%async_computation.4 | async-start | bytes 393216 | tf_op jit(solution)/shard_map/all_to_all | solution.py:125
where the time goes:
time: 207 us; the launch traced here: 206 us
  waiting for transfers between devices  95.4 us (46%)
  starting transfers between devices  37.5 us (18%)
  blocking collectives  35.3 us (17%)
  local copies, waits for them, and re-layouts  15.9 us (8%)
  matrix products  12.6 us (6%)
  other arithmetic  8.49 us (4%)
    all_to_all x1, waiting for transfers between devices, sum_at_owner(): lax.all_to_all(pieces, axis, split_axis=0, concat_axis=0, tiled=True)  39.2 us
    all_to_all x2, waiting for transfers between devices, from_everyone(): return lax.all_to_all(copies, axis, split_axis=0, concat_axis=0, tiled=True)  38.5 us
    all_to_all x1, blocking collectives, on_device(): lax.all_to_all(outgoing, 'ep', split_axis=0, concat_axis=0, tiled=True)  35.3 us
    all_to_all x1, waiting for transfers between devices, on_device(): lax.all_to_all(summed.reshape(groups, capacity, -1), 'ep', split_axis=0,...  17.6 us
    all_to_all x1, starting transfers between devices, on_device(): lax.all_to_all(summed.reshape(groups, capacity, -1), 'ep', split_axis=0,...  16.7 us
    all_to_all x2, starting transfers between devices, from_everyone(): return lax.all_to_all(copies, axis, split_axis=0, concat_axis=0, tiled=True)  10.7 us
    dot_general x1, matrix products, on_device(): jnp.dot(hidden, down_weight[0], preferred_element_type=jnp.float32)  7.13 us
    all_to_all x1, starting transfers between devices, sum_at_owner(): lax.all_to_all(pieces, axis, split_axis=0, concat_axis=0, tiled=True)  6.84 us
  transfers between devices with their start and end apart: 5, of which 3 were waited for; matrix products, arithmetic and copies ran while one was open for 9% of the time, Pallas kernels for 0%

commit v1 on v0

v1 whole, which is shorter than its diff:
```python
import jax
import jax.numpy as jnp
from jax import lax
from jax.experimental import pallas as pl
from jax.experimental.pallas import tpu as pltpu
from jax.sharding import PartitionSpec as P

norm_eps = 1e-06
F32 = jnp.float32
BF16 = jnp.bfloat16


def vmem_specs(count):
    return [pl.BlockSpec(memory_space=pltpu.VMEM)] * count


def call(body, outs, *operands):
    return pl.pallas_call(
        body,
        out_shape=tuple(jax.ShapeDtypeStruct(s, d) for s, d in outs),
        in_specs=vmem_specs(len(operands)),
        out_specs=tuple(vmem_specs(len(outs))),
        compiler_params=pltpu.CompilerParams(vmem_limit_bytes=20 * 1024 * 1024),
    )(*operands)


def column_of(row):
    size = row.shape[1]
    at = lax.broadcasted_iota(jnp.int32, (size, size), 0)
    to = lax.broadcasted_iota(jnp.int32, (size, size), 1)
    return jnp.sum(jnp.where(at == to, jnp.broadcast_to(row, (size, size)), 0.0), axis=1, keepdims=True)


def columns_of(row):
    return jnp.transpose(jnp.broadcast_to(row, (8, row.shape[1])))[:, 0:1]


def inv_rms(values):
    return lax.rsqrt(jnp.mean(values * values, axis=-1, keepdims=True) + norm_eps)


def prelude(groups, capacity, width, mix_ref, mgain_ref, wv_ref, wg_ref, exp_ref, egain_ref, routes_ref, logits_ref, out_ref, gated_ref, table_ref):
    rows_b = exp_ref.shape[0]
    routes = routes_ref[...]
    expert = lax.broadcasted_iota(jnp.int32, (groups, rows_b), 0)
    first = expert == routes[0:1, :]
    second = expert == routes[1:2, :]
    named = jnp.where(first | second, 1.0, 0.0)
    before = lax.broadcasted_iota(jnp.int32, (rows_b, rows_b), 0) < lax.broadcasted_iota(jnp.int32, (rows_b, rows_b), 1)
    earlier = jnp.dot(named.astype(BF16), jnp.where(before, 1.0, 0.0).astype(BF16), preferred_element_type=F32)
    slot = expert.astype(F32) * capacity + earlier
    slot_a = jnp.sum(jnp.where(first, slot, 0.0), axis=0, keepdims=True)
    slot_b = jnp.sum(jnp.where(second, slot, 0.0), axis=0, keepdims=True)
    logits = logits_ref[...]
    gap = logits[0:1, :] - logits[1:2, :]
    table_ref[...] = jnp.concatenate([slot_a, slot_b, jax.nn.sigmoid(gap), jax.nn.sigmoid(-gap), jnp.zeros((4, rows_b), F32)], axis=0)
    code = jnp.where(first | second, earlier, -1.0)
    place = lax.broadcasted_iota(jnp.int32, (groups, capacity, rows_b), 1).astype(F32)
    chosen = jnp.where(code[:, None, :] == place, 1.0, 0.0).reshape(groups * capacity, rows_b).astype(BF16)
    scale_b = inv_rms(exp_ref[...].astype(F32))
    start = pl.multiple_of(lax.axis_index("tp") * width, width)
    share = exp_ref[:, pl.ds(start, width)].astype(F32)
    normed_b = (share * scale_b * egain_ref[:, pl.ds(start, width)]).astype(BF16)
    out_ref[...] = jnp.dot(chosen, normed_b, preferred_element_type=F32).astype(BF16)
    rows = mix_ref[...].astype(F32)
    normed_a = (rows * inv_rms(rows) * mgain_ref[...]).astype(BF16)
    nt = (((1,), (1,)), ((), ()))
    value = lax.dot_general(wv_ref[...], normed_a, nt, preferred_element_type=F32)
    gate = lax.dot_general(wg_ref[...], normed_a, nt, preferred_element_type=F32)
    gated_ref[...] = (value * jax.nn.sigmoid(gate)).astype(BF16)


def conv_and_copies(arrived_ref, prev_ref, gated_ref, taps_ref, bias_ref, out_ref):
    count, _, width = out_ref.shape
    slots = arrived_ref.shape[0]
    taps = taps_ref[...]
    reach = taps.shape[1] - 1
    both = jnp.concatenate([prev_ref[...].astype(F32), gated_ref[...].astype(F32)], axis=1)
    span = both.shape[1]
    total = column_of(bias_ref[...]) + taps[:, reach : reach + 1] * both[:, width:]
    for k in range(reach):
        moved = pltpu.roll(both, reach - k, 1)
        total = total + taps[:, k : k + 1] * moved[:, span - width :]
    conv_out = total.astype(BF16)
    arrived = arrived_ref[...]
    for j in range(count):
        out_ref[j, :slots, :] = arrived
        out_ref[j, slots:, :] = conv_out


def experts_and_mixer(slots, block, x_ref, wg_ref, wu_ref, wd_ref, cgain_ref, cshift_ref, wo_ref, out_ref, mix_ref):
    count, _, width = x_ref.shape
    wg, wu, wd = wg_ref[0], wu_ref[0], wd_ref[0]
    for at in range(0, slots, block):
        rows = jnp.concatenate([x_ref[j, at : at + block, :] for j in range(count)], axis=1)
        gate = jnp.dot(rows, wg, preferred_element_type=F32)
        up = jnp.dot(rows, wu, preferred_element_type=F32)
        hidden = (gate * jax.nn.sigmoid(gate) * up).astype(BF16)
        part = jnp.dot(hidden, wd, preferred_element_type=F32).astype(BF16)
        for j in range(count):
            out_ref[j, at : at + block, :] = part[:, j * width : (j + 1) * width]
    values = jnp.concatenate([x_ref[j, slots:, :] for j in range(count)], axis=0).astype(F32)
    centered = values - jnp.mean(values, axis=0, keepdims=True)
    variance = jnp.mean(centered * centered, axis=0, keepdims=True)
    shaped = centered * lax.rsqrt(variance + norm_eps) * columns_of(cgain_ref[...]) + columns_of(cshift_ref[...])
    activated = (shaped * jax.nn.sigmoid(shaped)).astype(BF16)
    mix_ref[...] = lax.dot_general(activated, wo_ref[...], (((0,), (0,)), ((), ())), preferred_element_type=F32).astype(BF16)


def add_parts(parts_ref, out_ref):
    total = parts_ref[0].astype(F32)
    for j in range(1, parts_ref.shape[0]):
        total = total + parts_ref[j].astype(F32)
    out_ref[...] = total.astype(BF16)


def combine(back_ref, table_ref, out_ref):
    rows_b = out_ref.shape[0]
    slots = back_ref.shape[0]
    table = jnp.transpose(table_ref[...])
    place = lax.broadcasted_iota(jnp.int32, (rows_b, slots), 1).astype(F32)
    back = back_ref[...]
    total = None
    for j in range(2):
        pick = jnp.where(table[:, j : j + 1] == place, 1.0, 0.0).astype(BF16)
        term = jnp.dot(pick, back, preferred_element_type=F32) * table[:, 2 + j : 3 + j]
        total = term if total is None else total + term
    out_ref[...] = total.astype(BF16)


def exchange(blocks, axis):
    return lax.all_to_all(blocks, axis, split_axis=0, concat_axis=0, tiled=True)


def on_device(
    mixer_input,
    mixer_gain,
    glu_value_weight,
    glu_gate_weight,
    conv_taps,
    conv_bias,
    channel_gain,
    channel_shift,
    mixer_out_weight,
    expert_input,
    expert_gain,
    routes,
    route_logits,
    gate_weight,
    up_weight,
    down_weight,
):
    groups = lax.axis_size("ep")
    parts = lax.axis_size("tp")
    rows_b, features = expert_input.shape
    width = features // parts
    capacity = 3 * rows_b // groups
    slots = groups * capacity
    channels, tokens = glu_value_weight.shape[0], mixer_input.shape[0]

    def front(*refs):
        prelude(groups, capacity, width, *refs)

    outgoing, gated, table = call(
        front,
        [((slots, width), BF16), ((channels, tokens), BF16), ((8, rows_b), F32)],
        mixer_input,
        mixer_gain[None, :],
        glu_value_weight,
        glu_gate_weight,
        expert_input,
        expert_gain[None, :],
        routes.T,
        route_logits.T,
    )
    before = lax.ppermute(gated, "ep", [(i, i + 1) for i in range(groups - 1)])
    arrived = exchange(outgoing.reshape(groups, capacity, width), "ep").reshape(slots, width)
    (copies,) = call(
        conv_and_copies,
        [((parts, slots + channels, width), BF16)],
        arrived,
        before,
        gated,
        conv_taps,
        conv_bias[None, :],
    )
    gathered = exchange(copies, "tp")

    def middle(*refs):
        experts_and_mixer(slots, 256, *refs)

    partial, mixed = call(
        middle,
        [((parts, slots, width), BF16), ((tokens, width), BF16)],
        gathered,
        gate_weight,
        up_weight,
        down_weight,
        channel_gain[None, :],
        channel_shift[None, :],
        mixer_out_weight,
    )
    (summed,) = call(add_parts, [((slots, width), BF16)], exchange(partial, "tp"))
    returned = exchange(summed.reshape(groups, capacity, width), "ep").reshape(slots, width)
    (combined,) = call(combine, [((rows_b, width), BF16)], returned, table)
    return mixed, combined


def solution(mesh):
    in_specs = (
        P("ep", None),
        P(),
        P("tp", None),
        P("tp", None),
        P("tp", None),
        P("tp"),
        P(),
        P(),
        P(None, "tp"),
        P("ep", None),
        P(),
        P("ep", None),
        P("ep", None),
        P("ep", None, "tp"),
        P("ep", None, "tp"),
        P("ep", "tp", None),
    )
    out_specs = (P("ep", "tp"), P("ep", "tp"))
    return jax.shard_map(
        on_device, mesh=mesh, in_specs=in_specs, out_specs=out_specs, check_vma=False
    )
```

time: 207 us -> 165 us (0.80)
  waiting for transfers between devices: 95.4 us -> 15.1 us
  blocking collectives: 35.3 us -> 113 us
  starting transfers between devices: 37.5 us -> 20.3 us
  matrix products: 12.6 us -> 0 us
  other arithmetic: 8.49 us -> 0 us
  local copies, waits for them, and re-layouts: 15.9 us -> 8.23 us
  Pallas kernels: 0 us -> 7.36 us
    all_to_all x4 -> x1, waiting for transfers between devices: 95.4 us -> 14.3 us  [exchange(): return lax.all_to_all(blocks, axis, split_axis=0, concat_axis=0, tiled=True)]
    all_to_all x1 -> x3, blocking collectives: 35.3 us -> 113 us  [exchange(): return lax.all_to_all(blocks, axis, split_axis=0, concat_axis=0, tiled=True)]
    all_to_all x4 -> x1, starting transfers between devices: 34.2 us -> 16.7 us  [exchange(): return lax.all_to_all(blocks, axis, split_axis=0, concat_axis=0, tiled=True)]
    dot_general x5 -> x0, matrix products: 12.6 us -> none  [the longest x1 7.13 us: on_device(): jnp.dot(hidden, down_weight[0], preferred_element_type=jnp.float32)]
    unnamed x31 -> x32, local copies, waits for them, and re-layouts: 0.22 us -> 8.23 us
    pallas_call x0 -> x5, Pallas kernels: none -> 7.36 us  [call(): pl.pallas_call(body, out_shape=tuple((jax.ShapeDtypeStruct(s, d) for s, d...]
    reshape x3 -> x0, local copies, waits for them, and re-layouts: 4.65 us -> none  [the longest x1 4.37 us: in_blocks(): shard.reshape(*dims[:dim], count, dims[dim] // count, *dims[dim + 1:])]
    reduce_sum x6 -> x0, other arithmetic: 3.79 us -> none  [the longest x1 3.04 us: sum_at_owner(): return arrived.astype(jnp.float32).sum(axis=0)]
  transfers between devices with their start and end apart: 5 -> 2, of which waited for: 3 -> 2; matrix products, arithmetic and copies ran while one was open for 9% -> 0% of each run, Pallas kernels for 0% -> 0%
where the time goes in v1:
time: 165 us
  blocking collectives  113 us (68%)
  starting transfers between devices  20.3 us (12%)
  waiting for transfers between devices  15.1 us (9%)
  local copies, waits for them, and re-layouts  8.23 us (5%)
  Pallas kernels  7.36 us (4%)
    all_to_all x3, blocking collectives, exchange(): return lax.all_to_all(blocks, axis, split_axis=0, concat_axis=0, tiled=True)  113 us
    all_to_all x1, starting transfers between devices, exchange(): return lax.all_to_all(blocks, axis, split_axis=0, concat_axis=0, tiled=True)  16.7 us
    all_to_all x1, waiting for transfers between devices, exchange(): return lax.all_to_all(blocks, axis, split_axis=0, concat_axis=0, tiled=True)  14.3 us
    unnamed x32, local copies, waits for them, and re-layouts  8.23 us
    pallas_call x5, Pallas kernels, call(): pl.pallas_call(body, out_shape=tuple((jax.ShapeDtypeStruct(s, d) for s, d...  7.36 us
    ppermute x1, starting transfers between devices, on_device(): before = lax.ppermute(gated, 'ep', [(i, i + 1) for i in range(groups - 1)])  3.54 us
  transfers between devices with their start and end apart: 2, of which 2 were waited for; matrix products, arithmetic and copies ran while one was open for 0% of the time, Pallas kernels for 0%

profile of v1, /device:TPU:1, one launch (start us, length us, event | category | flops | bytes accessed | tf_op | source)
XLA Modules:
  0.0 164.8 jit_solution(9486089153817556529)
XLA Ops:
  0.6 0.0 copy-start
  0.6 1.2 copy-done
  1.9 1.0 copy-done.4
  2.9 0.9 copy-done.5
  3.8 0.9 copy-done.6
  4.7 0.7 copy-done.9
  5.4 0.7 copy-done.10
  6.1 0.7 copy-done.11
  6.8 0.7 copy-done.12
  7.5 1.4 shard_map.167
  8.9 16.7 %all-to-all-start = ((bf16[32,24,128]{2,1,0:T(8,128)(2,1)}), bf16[32,24,128]{2,1,0:T(8,128)(2,1)S(1)}, u32[]{:S(2)}, u32[]{:S(2)}) async-start(bf16[32,24,128]{2,1,0:T(8,128)(2,1)} %bitcast.4), calls=%async_computation | async-start | bytes 393216 | tf_op jit(solution)/shard_map/all_to_all | solution.py:132
  25.6 3.5 %collective-permute-start = (bf16[32,128]{1,0:T(8,128)(2,1)S(1)}, bf16[32,128]{1,0:T(8,128)(2,1)S(1)}, u32[]{:S(2)}, u32[]{:S(2)}) collective-permute-start(bf16[32,128]{1,0:T(8,128)(2,1)S(1)} %get-tuple-element.8.gated_ref), channel_id=1, source_target_pairs={{0,16},{16,32},{32,48},{48,64},{64,80},{80,96},{96,112},{112,128},... | collective-permute-start | bytes 24584 | tf_op jit(solution)/shard_map/ppermute | solution.py:176
  29.1 0.8 collective-permute-done.prev_ref
  29.9 14.3 %all-to-all-done = bf16[32,24,128]{2,1,0:T(8,128)(2,1)S(1)} async-done(((bf16[32,24,128]{2,1,0:T(8,128)(2,1)}), bf16[32,24,128]{2,1,0:T(8,128)(2,1)S(1)}, u32[]{:S(2)}, u32[]{:S(2)}) %all-to-all-start) | async-done | bytes 196640 | tf_op jit(solution)/shard_map/all_to_all | solution.py:132
  44.2 0.7 copy-done.8
  44.9 0.7 copy-done.15
  45.6 0.8 shard_map.168
  46.4 0.0 copy-start.1
  46.4 0.0 copy-start.2
  46.4 0.0 copy-start.3
  46.4 0.0 copy-start.7
  46.4 0.0 copy-start.13
  46.4 0.0 copy-start.14
  46.5 46.3 %all_to_all.20.refs_0_ = bf16[16,800,128]{2,1,0:T(8,128)(2,1)S(1)} all-to-all(bf16[16,800,128]{2,1,0:T(8,128)(2,1)S(1)} %shard_map.168), channel_id=1, replica_groups=mesh['ep'=32,'tp'=16] {'tp'}, dimensions={0} | all-to-all | bytes 6553600 | tf_op jit(solution)/shard_map/all_to_all | solution.py:132
  92.7 0.0 copy-done.1
  92.7 0.0 copy-done.2
  92.7 0.0 copy-done.3
  92.8 3.6 %shard_map.169 = (bf16[16,768,128]{2,1,0:T(8,128)(2,1)S(1)}, bf16[128,128]{1,0:T(8,128)(2,1)}) custom-call(bf16[16,800,128]{2,1,0:T(8,128)(2,1)S(1)} %all_to_all.20.refs_0_, bf16[1,2048,256]{2,1,0:T(8,128)(2,1)S(1)} %copy-done.1, bf16[1,2048,256]{2,1,0:T(8,128)(2,1)S(1)} %copy-done.2, bf16[1,256,2048]{2,1,0:T(8,128)(2,1)S(1)} %copy-done.3, ...), custom_call_target="tpu_custom_call" | custom-call | tf_op jit(solution)/shard_map/pallas_call | solution.py:18
  96.4 39.2 %all_to_all.21.parts_ref = bf16[16,768,128]{2,1,0:T(8,128)(2,1)S(1)} all-to-all(bf16[16,768,128]{2,1,0:T(8,128)(2,1)S(1)} %get-tuple-element.10), channel_id=1, replica_groups=mesh['ep'=32,'tp'=16] {'tp'}, dimensions={0} | all-to-all | bytes 6291456 | tf_op jit(solution)/shard_map/all_to_all | solution.py:132
  135.5 0.4 shard_map.170
  135.9 27.7 %all_to_all.22 = bf16[32,24,128]{2,1,0:T(8,128)(2,1)S(1)} all-to-all(bf16[32,24,128]{2,1,0:T(8,128)(2,1)S(1)} %bitcast.12), channel_id=1, replica_groups=mesh['ep'=32,'tp'=16] {'ep'}, dimensions={0} | all-to-all | bytes 393216 | tf_op jit(solution)/shard_map/all_to_all | solution.py:132
  163.6 1.2 shard_map.171
  (12 shorter events, 0.0 us)
Async XLA Ops:
  0.6 1.2 copy-start
  1.9 1.0 copy-start.4
  2.9 0.9 copy-start.5
  3.8 0.9 copy-start.6
  4.7 0.7 copy-start.9
  5.4 0.7 copy-start.10
  6.1 0.7 copy-start.11
  6.8 0.7 copy-start.12
  8.9 35.4 %all-to-all-start = ((bf16[32,24,128]{2,1,0:T(8,128)(2,1)}), bf16[32,24,128]{2,1,0:T(8,128)(2,1)S(1)}, u32[]{:S(2)}, u32[]{:S(2)}) async-start(bf16[32,24,128]{2,1,0:T(8,128)(2,1)} %bitcast.4), calls=%async_computation | async-start | bytes 393216 | tf_op jit(solution)/shard_map/all_to_all | solution.py:132
  25.6 4.3 %collective-permute-start = (bf16[32,128]{1,0:T(8,128)(2,1)S(1)}, bf16[32,128]{1,0:T(8,128)(2,1)S(1)}, u32[]{:S(2)}, u32[]{:S(2)}) collective-permute-start(bf16[32,128]{1,0:T(8,128)(2,1)S(1)} %get-tuple-element.8.gated_ref), channel_id=1, source_target_pairs={{0,16},{16,32},{32,48},{48,64},{64,80},{80,96},{96,112},{112,128},... | collective-permute-start | bytes 24584 | tf_op jit(solution)/shard_map/ppermute | solution.py:176
  44.2 0.7 copy-start.8
  44.9 0.7 copy-start.15
  46.4 46.4 %copy-start.1 = (bf16[1,2048,256]{2,1,0:T(8,128)(2,1)S(1)}, bf16[1,2048,256]{2,1,0:T(8,128)(2,1)}, u32[]{:S(2)}) copy-start(bf16[1,2048,256]{2,1,0:T(8,128)(2,1)} %refs_1_.1) | copy-start | bytes 3145732
  46.4 46.3 %copy-start.2 = (bf16[1,2048,256]{2,1,0:T(8,128)(2,1)S(1)}, bf16[1,2048,256]{2,1,0:T(8,128)(2,1)}, u32[]{:S(2)}) copy-start(bf16[1,2048,256]{2,1,0:T(8,128)(2,1)} %refs_2_.3) | copy-start | bytes 3145732
  46.4 46.3 %copy-start.3 = (bf16[1,256,2048]{2,1,0:T(8,128)(2,1)S(1)}, bf16[1,256,2048]{2,1,0:T(8,128)(2,1)}, u32[]{:S(2)}) copy-start(bf16[1,256,2048]{2,1,0:T(8,128)(2,1)} %refs_3_.3) | copy-start | bytes 3145732
  46.4 46.3 %copy-start.7 = (bf16[512,128]{1,0:T(8,128)(2,1)S(1)}, bf16[512,128]{1,0:T(8,128)(2,1)}, u32[]{:S(2)}) copy-start(bf16[512,128]{1,0:T(8,128)(2,1)} %refs_6_.1) | copy-start | bytes 393220
  46.4 46.3 %copy-start.13 = (f32[512]{0:T(512)S(1)}, f32[512]{0:T(512)}, u32[]{:S(2)}) copy-start(f32[512]{0:T(512)} %param.22) | copy-start | bytes 6148
  46.4 46.3 %copy-start.14 = (f32[512]{0:T(512)S(1)}, f32[512]{0:T(512)}, u32[]{:S(2)}) copy-start(f32[512]{0:T(512)} %param.23) | copy-start | bytes 6148

commit v2 on v1

--- a/solution.py
+++ b/solution.py
@@ -1,3 +1,5 @@
+import math
+
 import jax
 import jax.numpy as jnp
 from jax import lax
@@ -10,18 +12,40 @@
 BF16 = jnp.bfloat16
 
 
-def vmem_specs(count):
-    return [pl.BlockSpec(memory_space=pltpu.VMEM)] * count
-
-
-def call(body, outs, *operands):
+def whole(space, count):
+    return [pl.BlockSpec(memory_space=space)] * count
+
+
+def call(body, outs, *operands, source=pltpu.VMEM, scratch=()):
     return pl.pallas_call(
         body,
         out_shape=tuple(jax.ShapeDtypeStruct(s, d) for s, d in outs),
-        in_specs=vmem_specs(len(operands)),
-        out_specs=tuple(vmem_specs(len(outs))),
+        in_specs=whole(source, len(operands)),
+        out_specs=tuple(whole(pltpu.VMEM, len(outs))),
+        scratch_shapes=list(scratch),
         compiler_params=pltpu.CompilerParams(vmem_limit_bytes=20 * 1024 * 1024),
     )(*operands)
+
+
+def staged(body, outs, *operands):
+    count = len(operands)
+
+    def kernel(*refs):
+        sources, results = refs[:count], refs[count : count + len(outs)]
+        held, sems = refs[count + len(outs) : -1], refs[-1]
+        copies = [pltpu.make_async_copy(sources[i], held[i], sems.at[i]) for i in range(count)]
+        for copy in copies:
+            copy.start()
+
+        def load(i):
+            copies[i].wait()
+            return held[i]
+
+        body(load, *results)
+
+    scratch = [pltpu.VMEM(x.shape, x.dtype) for x in operands] + [pltpu.SemaphoreType.DMA((count,))]
+    pinned = [pltpu.with_memory_space_constraint(x, pltpu.HBM) for x in operands]
+    return call(kernel, outs, *pinned, source=pltpu.HBM, scratch=scratch)
 
 
 def column_of(row):
@@ -39,9 +63,10 @@
     return lax.rsqrt(jnp.mean(values * values, axis=-1, keepdims=True) + norm_eps)
 
 
-def prelude(groups, capacity, width, mix_ref, mgain_ref, wv_ref, wg_ref, exp_ref, egain_ref, routes_ref, logits_ref, out_ref, gated_ref, table_ref):
-    rows_b = exp_ref.shape[0]
-    routes = routes_ref[...]
+def dispatch(groups, capacity, width, load, out_ref, table_ref):
+    routes = load(0)[...]
+    logits = load(1)[...]
+    rows_b = routes.shape[1]
     expert = lax.broadcasted_iota(jnp.int32, (groups, rows_b), 0)
     first = expert == routes[0:1, :]
     second = expert == routes[1:2, :]
@@ -51,33 +76,38 @@
     slot = expert.astype(F32) * capacity + earlier
     slot_a = jnp.sum(jnp.where(first, slot, 0.0), axis=0, keepdims=True)
     slot_b = jnp.sum(jnp.where(second, slot, 0.0), axis=0, keepdims=True)
-    logits = logits_ref[...]
     gap = logits[0:1, :] - logits[1:2, :]
     table_ref[...] = jnp.concatenate([slot_a, slot_b, jax.nn.sigmoid(gap), jax.nn.sigmoid(-gap), jnp.zeros((4, rows_b), F32)], axis=0)
     code = jnp.where(first | second, earlier, -1.0)
     place = lax.broadcasted_iota(jnp.int32, (groups, capacity, rows_b), 1).astype(F32)
     chosen = jnp.where(code[:, None, :] == place, 1.0, 0.0).reshape(groups * capacity, rows_b).astype(BF16)
-    scale_b = inv_rms(exp_ref[...].astype(F32))
+    gain_ref, rows_ref = load(2), load(3)
+    scale = inv_rms(rows_ref[...].astype(F32))
     start = pl.multiple_of(lax.axis_index("tp") * width, width)
-    share = exp_ref[:, pl.ds(start, width)].astype(F32)
-    normed_b = (share * scale_b * egain_ref[:, pl.ds(start, width)]).astype(BF16)
-    out_ref[...] = jnp.dot(chosen, normed_b, preferred_element_type=F32).astype(BF16)
-    rows = mix_ref[...].astype(F32)
-    normed_a = (rows * inv_rms(rows) * mgain_ref[...]).astype(BF16)
+    share = rows_ref[:, pl.ds(start, width)].astype(F32)
+    normed = (share * scale * gain_ref[:, pl.ds(start, width)]).astype(BF16)
+    out_ref[...] = jnp.dot(chosen, normed, preferred_element_type=F32).astype(BF16)
+
+
+def mixer_front(load, gated_ref, taps_ref):
+    taps_ref[...] = jnp.concatenate([load(0)[...], column_of(load(1)[...])], axis=1)
+    gain_ref = load(2)
+    rows = load(3)[...].astype(F32)
+    normed = (rows * inv_rms(rows) * gain_ref[...]).astype(BF16)
     nt = (((1,), (1,)), ((), ()))
-    value = lax.dot_general(wv_ref[...], normed_a, nt, preferred_element_type=F32)
-    gate = lax.dot_general(wg_ref[...], normed_a, nt, preferred_element_type=F32)
+    value = lax.dot_general(load(4)[...], normed, nt, preferred_element_type=F32)
+    gate = lax.dot_general(load(5)[...], normed, nt, preferred_element_type=F32)
     gated_ref[...] = (value * jax.nn.sigmoid(gate)).astype(BF16)
 
 
-def conv_and_copies(arrived_ref, prev_ref, gated_ref, taps_ref, bias_ref, out_ref):
+def conv_and_copies(arrived_ref, prev_ref, gated_ref, taps_ref, out_ref):
     count, _, width = out_ref.shape
     slots = arrived_ref.shape[0]
     taps = taps_ref[...]
-    reach = taps.shape[1] - 1
+    reach = taps.shape[1] - 2
     both = jnp.concatenate([prev_ref[...].astype(F32), gated_ref[...].astype(F32)], axis=1)
     span = both.shape[1]
-    total = column_of(bias_ref[...]) + taps[:, reach : reach + 1] * both[:, width:]
+    total = taps[:, reach + 1 :] + taps[:, reach : reach + 1] * both[:, width:]
     for k in range(reach):
         moved = pltpu.roll(both, reach - k, 1)
         total = total + taps[:, k : k + 1] * moved[:, span - width :]
@@ -88,18 +118,25 @@
         out_ref[j, slots:, :] = conv_out
 
 
-def experts_and_mixer(slots, block, x_ref, wg_ref, wu_ref, wd_ref, cgain_ref, cshift_ref, wo_ref, out_ref, mix_ref):
+def swapped(j, side, swap):
+    return jnp.where(swap, (j % side) * side + j // side, j)
+
+
+def experts_and_mixer(slots, block, side, x_ref, wg_ref, wu_ref, wd_ref, cgain_ref, cshift_ref, wo_ref, out_ref, mix_ref):
     count, _, width = x_ref.shape
+    odd = lax.axis_index("ep") % 2 == 1
+    came = [swapped(j, side, odd) for j in range(count)]
+    goes = [swapped(j, side, ~odd) for j in range(count)]
     wg, wu, wd = wg_ref[0], wu_ref[0], wd_ref[0]
     for at in range(0, slots, block):
-        rows = jnp.concatenate([x_ref[j, at : at + block, :] for j in range(count)], axis=1)
+        rows = jnp.concatenate([x_ref[came[j], at : at + block, :] for j in range(count)], axis=1)
         gate = jnp.dot(rows, wg, preferred_element_type=F32)
         up = jnp.dot(rows, wu, preferred_element_type=F32)
         hidden = (gate * jax.nn.sigmoid(gate) * up).astype(BF16)
         part = jnp.dot(hidden, wd, preferred_element_type=F32).astype(BF16)
         for j in range(count):
-            out_ref[j, at : at + block, :] = part[:, j * width : (j + 1) * width]
-    values = jnp.concatenate([x_ref[j, slots:, :] for j in range(count)], axis=0).astype(F32)
+            out_ref[goes[j], at : at + block, :] = part[:, j * width : (j + 1) * width]
+    values = jnp.concatenate([x_ref[came[j], slots:, :] for j in range(count)], axis=0).astype(F32)
     centered = values - jnp.mean(values, axis=0, keepdims=True)
     variance = jnp.mean(centered * centered, axis=0, keepdims=True)
     shaped = centered * lax.rsqrt(variance + norm_eps) * columns_of(cgain_ref[...]) + columns_of(cshift_ref[...])
@@ -128,8 +165,17 @@
     out_ref[...] = total.astype(BF16)
 
 
-def exchange(blocks, axis):
-    return lax.all_to_all(blocks, axis, split_axis=0, concat_axis=0, tiled=True)
+def exchange(blocks, axis, members=None):
+    return lax.all_to_all(blocks, axis, split_axis=0, concat_axis=0, tiled=True, axis_index_groups=members)
+
+
+def plane_groups(groups, side, first):
+    members = []
+    for e in range(groups):
+        along_x = (e % 2 == 0) == first
+        for a in range(side):
+            members.append([e * side * side + (a * side + b if along_x else b * side + a) for b in range(side)])
+    return members
 
 
 def on_device(
@@ -158,41 +204,45 @@
     slots = groups * capacity
     channels, tokens = glu_value_weight.shape[0], mixer_input.shape[0]
 
+    side = math.isqrt(parts)
+    plane = ("ep", "tp")
+    line_one, line_two = plane_groups(groups, side, True), plane_groups(groups, side, False)
+
     def front(*refs):
-        prelude(groups, capacity, width, *refs)
-
-    outgoing, gated, table = call(
+        dispatch(groups, capacity, width, *refs)
+
+    outgoing, table = staged(
         front,
-        [((slots, width), BF16), ((channels, tokens), BF16), ((8, rows_b), F32)],
+        [((slots, width), BF16), ((8, rows_b), F32)],
+        routes.T,
+        route_logits.T,
+        expert_gain[None, :],
+        expert_input,
+    )
+    gated, taps = staged(
+        mixer_front,
+        [((channels, tokens), BF16), ((channels, conv_taps.shape[1] + 1), F32)],
+        conv_taps,
+        conv_bias[None, :],
+        mixer_gain[None, :],
         mixer_input,
-        mixer_gain[None, :],
         glu_value_weight,
         glu_gate_weight,
-        expert_input,
-        expert_gain[None, :],
-        routes.T,
-        route_logits.T,
     )
     before = lax.ppermute(gated, "ep", [(i, i + 1) for i in range(groups - 1)])
     arrived = exchange(outgoing.reshape(groups, capacity, width), "ep").reshape(slots, width)
-    (copies,) = call(
-        conv_and_copies,
-        [((parts, slots + channels, width), BF16)],
-        arrived,
-        before,
-        gated,
-        conv_taps,
-        conv_bias[None, :],
-    )
-    gathered = exchange(copies, "tp")
+    held = slots + channels
+    (copies,) = call(conv_and_copies, [((side, held, width), BF16)], arrived, before, gated, taps)
+    line = exchange(copies, plane, line_one).reshape(side * held, width)
+    gathered = exchange(jnp.broadcast_to(line, (side, *line.shape)), plane, line_two)
 
     def middle(*refs):
-        experts_and_mixer(slots, 256, *refs)
+        experts_and_mixer(slots, 256, side, *refs)
 
     partial, mixed = call(
         middle,
         [((parts, slots, width), BF16), ((tokens, width), BF16)],
-        gathered,
+        gathered.reshape(parts, held, width),
         gate_weight,
         up_weight,
         down_weight,
@@ -200,7 +250,8 @@
         channel_shift[None, :],
         mixer_out_weight,
     )
-    (summed,) = call(add_parts, [((slots, width), BF16)], exchange(partial, "tp"))
+    (line_sum,) = call(add_parts, [((side * slots, width), BF16)], exchange(partial.reshape(side, side * slots, width), plane, line_one))
+    (summed,) = call(add_parts, [((slots, width), BF16)], exchange(line_sum.reshape(side, slots, width), plane, line_two))
     returned = exchange(summed.reshape(groups, capacity, width), "ep").reshape(slots, width)
     (combined,) = call(combine, [((rows_b, width), BF16)], returned, table)
     return mixed, combined

time: 165 us -> 146 us (0.88)
  blocking collectives: 113 us -> 101 us
  local copies, waits for them, and re-layouts: 8.23 us -> 0.46 us
  Pallas kernels: 7.36 us -> 10.4 us
  waiting for transfers between devices: 15.1 us -> 13.1 us
    all_to_all x3 -> x5, blocking collectives: 113 us -> 101 us  [exchange(): lax.all_to_all(blocks, axis, split_axis=0, concat_axis=0, tiled=True, axi...]
    unnamed x32 -> x12, local copies, waits for them, and re-layouts: 8.23 us -> 0.04 us
    pallas_call x5 -> x7, Pallas kernels: 7.36 us -> 10.4 us  [call(): pl.pallas_call(body, out_shape=tuple((jax.ShapeDtypeStruct(s, d) for s, d...]
    all_to_all x1, waiting for transfers between devices: 14.3 us -> 12.3 us  [exchange(): lax.all_to_all(blocks, axis, split_axis=0, concat_axis=0, tiled=True, axi...]
  transfers between devices with their start and end apart: 2 -> 2, of which waited for: 2 -> 2; matrix products, arithmetic and copies ran while one was open for 0% -> 0% of each run, Pallas kernels for 0% -> 1%
where the time goes in v2:
time: 146 us
  blocking collectives  101 us (69%)
  starting transfers between devices  20.3 us (14%)
  waiting for transfers between devices  13.1 us (9%)
  Pallas kernels  10.4 us (7%)
    all_to_all x5, blocking collectives, exchange(): lax.all_to_all(blocks, axis, split_axis=0, concat_axis=0, tiled=True, axi...  101 us
    all_to_all x1, starting transfers between devices, exchange(): lax.all_to_all(blocks, axis, split_axis=0, concat_axis=0, tiled=True, axi...  16.7 us
    all_to_all x1, waiting for transfers between devices, exchange(): lax.all_to_all(blocks, axis, split_axis=0, concat_axis=0, tiled=True, axi...  12.3 us
    pallas_call x7, Pallas kernels, call(): pl.pallas_call(body, out_shape=tuple((jax.ShapeDtypeStruct(s, d) for s, d...  10.4 us
    ppermute x1, starting transfers between devices, on_device(): before = lax.ppermute(gated, 'ep', [(i, i + 1) for i in range(groups - 1)])  3.54 us
  transfers between devices with their start and end apart: 2, of which 2 were waited for; matrix products, arithmetic and copies ran while one was open for 0% of the time, Pallas kernels for 1%

profile of v2, /device:TPU:1, one launch (start us, length us, event | category | flops | bytes accessed | tf_op | source)
XLA Modules:
  0.0 145.7 jit_solution(17016596069752527190)
XLA Ops:
  0.6 2.5 %shard_map.167 = (bf16[768,128]{1,0:T(8,128)(2,1)}, f32[8,256]{1,0:T(8,128)S(1)}) custom-call(s32[2,256]{1,0:T(2,128)} %bitcast.26, f32[2,256]{1,0:T(2,128)} %bitcast.27, f32[1,2048]{1,0:T(1,128)} %bitcast.24, bf16[256,2048]{1,0:T(8,128)(2,1)} %refs_3_.3), custom_call_target="tpu_custom_call" | custom-call | tf_op jit(solution)/shard_map/pallas_call | solution.py:20
  3.2 16.7 %all-to-all-start = ((bf16[32,24,128]{2,1,0:T(8,128)(2,1)}), bf16[32,24,128]{2,1,0:T(8,128)(2,1)S(1)}, u32[]{:S(2)}, u32[]{:S(2)}) async-start(bf16[32,24,128]{2,1,0:T(8,128)(2,1)} %bitcast.3), calls=%async_computation | async-start | bytes 393216 | tf_op jit(solution)/shard_map/all_to_all | solution.py:169
  19.9 2.1 %shard_map.168 = (bf16[32,128]{1,0:T(8,128)(2,1)S(1)}, f32[32,32]{1,0:T(8,128)S(1)}) custom-call(f32[32,31]{1,0:T(8,128)} %refs_0_.1, f32[1,32]{1,0:T(1,128)} %bitcast.28, f32[1,2048]{1,0:T(1,128)} %bitcast.25, bf16[128,2048]{1,0:T(8,128)(2,1)} %refs_3_.4, bf16[32,2048]{1,0:T(8,128)(2,1)} %refs_4_.1, bf16[32,2048]{1,0:T(8,128)(2,1)} %refs_5_.1), custom_call_target="tpu_custom_call" | custom-call | tf_op jit(solution)/shard_map/pallas_call | solution.py:20
  22.1 3.5 %collective-permute-start = (bf16[32,128]{1,0:T(8,128)(2,1)S(1)}, bf16[32,128]{1,0:T(8,128)(2,1)S(1)}, u32[]{:S(2)}, u32[]{:S(2)}) collective-permute-start(bf16[32,128]{1,0:T(8,128)(2,1)S(1)} %get-tuple-element.9.gated_ref), channel_id=1, source_target_pairs={{0,16},{16,32},{32,48},{48,64},{64,80},{80,96},{96,112},{112,128},... | collective-permute-start | bytes 24584 | tf_op jit(solution)/shard_map/ppermute | solution.py:232
  25.6 0.8 collective-permute-done.prev_ref
  26.4 12.3 %all-to-all-done = bf16[32,24,128]{2,1,0:T(8,128)(2,1)S(1)} async-done(((bf16[32,24,128]{2,1,0:T(8,128)(2,1)}), bf16[32,24,128]{2,1,0:T(8,128)(2,1)S(1)}, u32[]{:S(2)}, u32[]{:S(2)}) %all-to-all-start) | async-done | bytes 196640 | tf_op jit(solution)/shard_map/all_to_all | solution.py:169
  38.7 0.5 shard_map.169
  39.2 12.6 %all_to_all.30 = bf16[4,800,128]{2,1,0:T(8,128)(2,1)S(1)} all-to-all(bf16[4,800,128]{2,1,0:T(8,128)(2,1)S(1)} %shard_map.169), channel_id=1, replica_groups={{0,1,2,3},{4,5,6,7},{8,9,10,11},{12,13,14,15},{16,20,24,28},{17,21,25,2..., dimensions={0} | all-to-all | bytes 1638400 | tf_op jit(solution)/shard_map/all_to_all | solution.py:169
  51.8 0.4 broadcast_in_dim.21
  52.2 0.0 copy-start
  52.2 0.0 copy-start.1
  52.2 0.0 copy-start.2
  52.3 0.0 copy-start.3
  52.3 0.0 copy-start.4
  52.3 0.0 copy-start.5
  52.3 26.0 %all_to_all.31 = bf16[4,3200,128]{2,1,0:T(8,128)(2,1)S(1)} all-to-all(bf16[4,3200,128]{2,1,0:T(8,128)(2,1)S(1)} %broadcast_in_dim.21), channel_id=1, replica_groups={{0,4,8,12},{1,5,9,13},{2,6,10,14},{3,7,11,15},{16,17,18,19},{20,21,22,2..., dimensions={0} | all-to-all | bytes 6553600 | tf_op jit(solution)/shard_map/all_to_all | solution.py:169
  78.3 0.0 copy-done
  78.3 0.0 copy-done.1
  78.3 0.0 copy-done.2
  78.3 0.0 copy-done.3
  78.3 0.0 copy-done.4
  78.3 0.0 copy-done.5
  78.3 3.6 %shard_map.170 = (bf16[16,768,128]{2,1,0:T(8,128)(2,1)S(1)}, bf16[128,128]{1,0:T(8,128)(2,1)}) custom-call(bf16[16,800,128]{2,1,0:T(8,128)(2,1)S(1)} %bitcast.15, bf16[1,2048,256]{2,1,0:T(8,128)(2,1)S(1)} %copy-done, bf16[1,2048,256]{2,1,0:T(8,128)(2,1)S(1)} %copy-done.1, bf16[1,256,2048]{2,1,0:T(8,128)(2,1)S(1)} %copy-done.2, f32[1,512]{1,0:T(1,128)S(1)} %bitcast.21, ...), custom_call_target="tpu_custom_call" | custom-call | tf_op jit(solution)/shard_map/pallas_call | solution.py:20
  81.9 23.8 %all_to_all.32.parts_ref = bf16[4,3072,128]{2,1,0:T(8,128)(2,1)S(1)} all-to-all(bf16[4,3072,128]{2,1,0:T(8,128)(2,1)S(1)} %bitcast.16), channel_id=1, replica_groups={{0,1,2,3},{4,5,6,7},{8,9,10,11},{12,13,14,15},{16,20,24,28},{17,21,25,2..., dimensions={0} | all-to-all | bytes 6291456 | tf_op jit(solution)/shard_map/all_to_all | solution.py:169
  105.6 0.4 shard_map.171
  106.0 10.7 %all_to_all.33.parts_ref = bf16[4,768,128]{2,1,0:T(8,128)(2,1)S(1)} all-to-all(bf16[4,768,128]{2,1,0:T(8,128)(2,1)S(1)} %bitcast.17), channel_id=1, replica_groups={{0,4,8,12},{1,5,9,13},{2,6,10,14},{3,7,11,15},{16,17,18,19},{20,21,22,2..., dimensions={0} | all-to-all | bytes 1572864 | tf_op jit(solution)/shard_map/all_to_all | solution.py:169
  116.8 0.1 shard_map.172
  116.9 27.6 %all_to_all.34 = bf16[32,24,128]{2,1,0:T(8,128)(2,1)S(1)} all-to-all(bf16[32,24,128]{2,1,0:T(8,128)(2,1)S(1)} %bitcast.20), channel_id=1, replica_groups=mesh['ep'=32,'tp'=16] {'ep'}, dimensions={0} | all-to-all | bytes 393216 | tf_op jit(solution)/shard_map/all_to_all | solution.py:169
  144.5 1.2 shard_map.173
Async XLA Ops:
  3.2 35.5 %all-to-all-start = ((bf16[32,24,128]{2,1,0:T(8,128)(2,1)}), bf16[32,24,128]{2,1,0:T(8,128)(2,1)S(1)}, u32[]{:S(2)}, u32[]{:S(2)}) async-start(bf16[32,24,128]{2,1,0:T(8,128)(2,1)} %bitcast.3), calls=%async_computation | async-start | bytes 393216 | tf_op jit(solution)/shard_map/all_to_all | solution.py:169
  22.1 4.3 %collective-permute-start = (bf16[32,128]{1,0:T(8,128)(2,1)S(1)}, bf16[32,128]{1,0:T(8,128)(2,1)S(1)}, u32[]{:S(2)}, u32[]{:S(2)}) collective-permute-start(bf16[32,128]{1,0:T(8,128)(2,1)S(1)} %get-tuple-element.9.gated_ref), channel_id=1, source_target_pairs={{0,16},{16,32},{32,48},{48,64},{64,80},{80,96},{96,112},{112,128},... | collective-permute-start | bytes 24584 | tf_op jit(solution)/shard_map/ppermute | solution.py:232
  52.2 26.0 %copy-start = (bf16[1,2048,256]{2,1,0:T(8,128)(2,1)S(1)}, bf16[1,2048,256]{2,1,0:T(8,128)(2,1)}, u32[]{:S(2)}) copy-start(bf16[1,2048,256]{2,1,0:T(8,128)(2,1)} %refs_1_.1) | copy-start | bytes 3145732
  52.2 26.0 %copy-start.1 = (bf16[1,2048,256]{2,1,0:T(8,128)(2,1)S(1)}, bf16[1,2048,256]{2,1,0:T(8,128)(2,1)}, u32[]{:S(2)}) copy-start(bf16[1,2048,256]{2,1,0:T(8,128)(2,1)} %refs_2_.1) | copy-start | bytes 3145732
  52.2 26.0 %copy-start.2 = (bf16[1,256,2048]{2,1,0:T(8,128)(2,1)S(1)}, bf16[1,256,2048]{2,1,0:T(8,128)(2,1)}, u32[]{:S(2)}) copy-start(bf16[1,256,2048]{2,1,0:T(8,128)(2,1)} %refs_3_.5) | copy-start | bytes 3145732
  52.3 26.0 %copy-start.3 = (bf16[512,128]{1,0:T(8,128)(2,1)S(1)}, bf16[512,128]{1,0:T(8,128)(2,1)}, u32[]{:S(2)}) copy-start(bf16[512,128]{1,0:T(8,128)(2,1)} %refs_6_.1) | copy-start | bytes 393220
  52.3 26.0 %copy-start.4 = (f32[512]{0:T(512)S(1)}, f32[512]{0:T(512)}, u32[]{:S(2)}) copy-start(f32[512]{0:T(512)} %param.22) | copy-start | bytes 6148
  52.3 26.0 %copy-start.5 = (f32[512]{0:T(512)S(1)}, f32[512]{0:T(512)}, u32[]{:S(2)}) copy-start(f32[512]{0:T(512)} %param.23) | copy-start | bytes 6148

commit v3 on v2

--- a/solution.py
+++ b/solution.py
@@ -118,25 +118,34 @@
         out_ref[j, slots:, :] = conv_out
 
 
-def swapped(j, side, swap):
-    return jnp.where(swap, (j % side) * side + j // side, j)
+def plane_places(side):
+    odd = lax.axis_index("ep") % 2
+    here = lax.axis_index("tp")
+
+    def steps(at):
+        base = (at - odd + side) % side // 2 * 2
+        return [(k + 1 - odd - base + side) % side for k in range(side)]
+
+    down, across = steps(here // side), steps(here % side)
+    return [
+        ((down[j // side] // 2) * 2 + across[j % side] // 2) * 4 + (down[j // side] % 2) * 2 + across[j % side] % 2
+        for j in range(side * side)
+    ]
 
 
 def experts_and_mixer(slots, block, side, x_ref, wg_ref, wu_ref, wd_ref, cgain_ref, cshift_ref, wo_ref, out_ref, mix_ref):
     count, _, width = x_ref.shape
-    odd = lax.axis_index("ep") % 2 == 1
-    came = [swapped(j, side, odd) for j in range(count)]
-    goes = [swapped(j, side, ~odd) for j in range(count)]
+    place = plane_places(side)
     wg, wu, wd = wg_ref[0], wu_ref[0], wd_ref[0]
     for at in range(0, slots, block):
-        rows = jnp.concatenate([x_ref[came[j], at : at + block, :] for j in range(count)], axis=1)
+        rows = jnp.concatenate([x_ref[place[j], at : at + block, :] for j in range(count)], axis=1)
         gate = jnp.dot(rows, wg, preferred_element_type=F32)
         up = jnp.dot(rows, wu, preferred_element_type=F32)
         hidden = (gate * jax.nn.sigmoid(gate) * up).astype(BF16)
         part = jnp.dot(hidden, wd, preferred_element_type=F32).astype(BF16)
         for j in range(count):
-            out_ref[goes[j], at : at + block, :] = part[:, j * width : (j + 1) * width]
-    values = jnp.concatenate([x_ref[came[j], slots:, :] for j in range(count)], axis=0).astype(F32)
+            out_ref[place[j], at : at + block, :] = part[:, j * width : (j + 1) * width]
+    values = jnp.concatenate([x_ref[place[j], slots:, :] for j in range(count)], axis=0).astype(F32)
     centered = values - jnp.mean(values, axis=0, keepdims=True)
     variance = jnp.mean(centered * centered, axis=0, keepdims=True)
     shaped = centered * lax.rsqrt(variance + norm_eps) * columns_of(cgain_ref[...]) + columns_of(cshift_ref[...])
@@ -169,12 +178,18 @@
     return lax.all_to_all(blocks, axis, split_axis=0, concat_axis=0, tiled=True, axis_index_groups=members)
 
 
-def plane_groups(groups, side, first):
+def plane_groups(groups, side, turned):
+    half = side // 2
     members = []
     for e in range(groups):
-        along_x = (e % 2 == 0) == first
-        for a in range(side):
-            members.append([e * side * side + (a * side + b if along_x else b * side + a) for b in range(side)])
+        shift = (e + turned) % 2
+        for by in range(half):
+            for bx in range(half):
+                members.append([
+                    e * side * side + (2 * by + oy + shift) % side * side + (2 * bx + ox + shift) % side
+                    for oy in range(2)
+                    for ox in range(2)
+                ])
     return members
 
 
@@ -206,7 +221,7 @@
 
     side = math.isqrt(parts)
     plane = ("ep", "tp")
-    line_one, line_two = plane_groups(groups, side, True), plane_groups(groups, side, False)
+    inner, outer = plane_groups(groups, side, 1), plane_groups(groups, side, 0)
 
     def front(*refs):
         dispatch(groups, capacity, width, *refs)
@@ -233,8 +248,8 @@
     arrived = exchange(outgoing.reshape(groups, capacity, width), "ep").reshape(slots, width)
     held = slots + channels
     (copies,) = call(conv_and_copies, [((side, held, width), BF16)], arrived, before, gated, taps)
-    line = exchange(copies, plane, line_one).reshape(side * held, width)
-    gathered = exchange(jnp.broadcast_to(line, (side, *line.shape)), plane, line_two)
+    block = exchange(copies, plane, inner).reshape(side * held, width)
+    gathered = exchange(jnp.broadcast_to(block, (side, *block.shape)), plane, outer)
 
     def middle(*refs):
         experts_and_mixer(slots, 256, side, *refs)
@@ -250,8 +265,8 @@
         channel_shift[None, :],
         mixer_out_weight,
     )
-    (line_sum,) = call(add_parts, [((side * slots, width), BF16)], exchange(partial.reshape(side, side * slots, width), plane, line_one))
-    (summed,) = call(add_parts, [((slots, width), BF16)], exchange(line_sum.reshape(side, slots, width), plane, line_two))
+    (block_sum,) = call(add_parts, [((side * slots, width), BF16)], exchange(partial.reshape(side, side * slots, width), plane, outer))
+    (summed,) = call(add_parts, [((slots, width), BF16)], exchange(block_sum.reshape(side, slots, width), plane, inner))
     returned = exchange(summed.reshape(groups, capacity, width), "ep").reshape(slots, width)
     (combined,) = call(combine, [((rows_b, width), BF16)], returned, table)
     return mixed, combined

time: 146 us -> 144 us (0.986)
  blocking collectives: 101 us -> 98.5 us
    all_to_all x5, blocking collectives: 101 us -> 98.5 us  [exchange(): lax.all_to_all(blocks, axis, split_axis=0, concat_axis=0, tiled=True, axi...]
where the time goes in v3:
time: 144 us
  blocking collectives  98.5 us (68%)
  starting transfers between devices  20.3 us (14%)
  waiting for transfers between devices  13.1 us (9%)
  Pallas kernels  10.5 us (7%)
    all_to_all x5, blocking collectives, exchange(): lax.all_to_all(blocks, axis, split_axis=0, concat_axis=0, tiled=True, axi...  98.5 us
    all_to_all x1, starting transfers between devices, exchange(): lax.all_to_all(blocks, axis, split_axis=0, concat_axis=0, tiled=True, axi...  16.7 us
    all_to_all x1, waiting for transfers between devices, exchange(): lax.all_to_all(blocks, axis, split_axis=0, concat_axis=0, tiled=True, axi...  12.3 us
    pallas_call x7, Pallas kernels, call(): pl.pallas_call(body, out_shape=tuple((jax.ShapeDtypeStruct(s, d) for s, d...  10.5 us
    ppermute x1, starting transfers between devices, on_device(): before = lax.ppermute(gated, 'ep', [(i, i + 1) for i in range(groups - 1)])  3.54 us
  transfers between devices with their start and end apart: 2, of which 2 were waited for; matrix products, arithmetic and copies ran while one was open for 0% of the time, Pallas kernels for 1%

profile of v3, /device:TPU:1, one launch (start us, length us, event | category | flops | bytes accessed | tf_op | source)
XLA Modules:
  0.0 143.5 jit_solution(1333902307675377254)
XLA Ops:
  0.6 2.5 %shard_map.167 = (bf16[768,128]{1,0:T(8,128)(2,1)}, f32[8,256]{1,0:T(8,128)S(1)}) custom-call(s32[2,256]{1,0:T(2,128)} %bitcast.26, f32[2,256]{1,0:T(2,128)} %bitcast.27, f32[1,2048]{1,0:T(1,128)} %bitcast.24, bf16[256,2048]{1,0:T(8,128)(2,1)} %refs_3_.3), custom_call_target="tpu_custom_call" | custom-call | tf_op jit(solution)/shard_map/pallas_call | solution.py:20
  3.2 16.7 %all-to-all-start = ((bf16[32,24,128]{2,1,0:T(8,128)(2,1)}), bf16[32,24,128]{2,1,0:T(8,128)(2,1)S(1)}, u32[]{:S(2)}, u32[]{:S(2)}) async-start(bf16[32,24,128]{2,1,0:T(8,128)(2,1)} %bitcast.3), calls=%async_computation | async-start | bytes 393216 | tf_op jit(solution)/shard_map/all_to_all | solution.py:178
  19.9 2.1 %shard_map.168 = (bf16[32,128]{1,0:T(8,128)(2,1)S(1)}, f32[32,32]{1,0:T(8,128)S(1)}) custom-call(f32[32,31]{1,0:T(8,128)} %refs_0_.1, f32[1,32]{1,0:T(1,128)} %bitcast.28, f32[1,2048]{1,0:T(1,128)} %bitcast.25, bf16[128,2048]{1,0:T(8,128)(2,1)} %refs_3_.4, bf16[32,2048]{1,0:T(8,128)(2,1)} %refs_4_.1, bf16[32,2048]{1,0:T(8,128)(2,1)} %refs_5_.1), custom_call_target="tpu_custom_call" | custom-call | tf_op jit(solution)/shard_map/pallas_call | solution.py:20
  22.1 3.5 %collective-permute-start = (bf16[32,128]{1,0:T(8,128)(2,1)S(1)}, bf16[32,128]{1,0:T(8,128)(2,1)S(1)}, u32[]{:S(2)}, u32[]{:S(2)}) collective-permute-start(bf16[32,128]{1,0:T(8,128)(2,1)S(1)} %get-tuple-element.9.gated_ref), channel_id=1, source_target_pairs={{0,16},{16,32},{32,48},{48,64},{64,80},{80,96},{96,112},{112,128},... | collective-permute-start | bytes 24584 | tf_op jit(solution)/shard_map/ppermute | solution.py:247
  25.6 0.8 collective-permute-done.prev_ref
  26.4 12.3 %all-to-all-done = bf16[32,24,128]{2,1,0:T(8,128)(2,1)S(1)} async-done(((bf16[32,24,128]{2,1,0:T(8,128)(2,1)}), bf16[32,24,128]{2,1,0:T(8,128)(2,1)S(1)}, u32[]{:S(2)}, u32[]{:S(2)}) %all-to-all-start) | async-done | bytes 196640 | tf_op jit(solution)/shard_map/all_to_all | solution.py:178
  38.7 0.5 shard_map.169
  39.2 11.4 %all_to_all.30 = bf16[4,800,128]{2,1,0:T(8,128)(2,1)S(1)} all-to-all(bf16[4,800,128]{2,1,0:T(8,128)(2,1)S(1)} %shard_map.169), channel_id=1, replica_groups={{5,6,9,10},{7,4,11,8},{13,14,1,2},{15,12,3,0},{16,17,20,21},{18,19,22,2..., dimensions={0} | all-to-all | bytes 1638400 | tf_op jit(solution)/shard_map/all_to_all | solution.py:178
  50.6 0.4 broadcast_in_dim.21
  51.0 0.0 copy-start
  51.0 0.0 copy-start.1
  51.0 0.0 copy-start.2
  51.0 0.0 copy-start.3
  51.0 0.0 copy-start.4
  51.1 0.0 copy-start.5
  51.1 25.1 %all_to_all.31 = bf16[4,3200,128]{2,1,0:T(8,128)(2,1)S(1)} all-to-all(bf16[4,3200,128]{2,1,0:T(8,128)(2,1)S(1)} %broadcast_in_dim.21), channel_id=1, replica_groups={{0,1,4,5},{2,3,6,7},{8,9,12,13},{10,11,14,15},{21,22,25,26},{23,20,27,2..., dimensions={0} | all-to-all | bytes 6553600 | tf_op jit(solution)/shard_map/all_to_all | solution.py:178
  76.2 0.0 copy-done
  76.2 0.0 copy-done.1
  76.2 0.0 copy-done.2
  76.2 0.0 copy-done.3
  76.2 0.0 copy-done.4
  76.2 0.0 copy-done.5
  76.2 3.6 %shard_map.170 = (bf16[16,768,128]{2,1,0:T(8,128)(2,1)S(1)}, bf16[128,128]{1,0:T(8,128)(2,1)}) custom-call(bf16[16,800,128]{2,1,0:T(8,128)(2,1)S(1)} %bitcast.15, bf16[1,2048,256]{2,1,0:T(8,128)(2,1)S(1)} %copy-done, bf16[1,2048,256]{2,1,0:T(8,128)(2,1)S(1)} %copy-done.1, bf16[1,256,2048]{2,1,0:T(8,128)(2,1)S(1)} %copy-done.2, f32[1,512]{1,0:T(1,128)S(1)} %bitcast.21, ...), custom_call_target="tpu_custom_call" | custom-call | tf_op jit(solution)/shard_map/pallas_call | solution.py:20
  79.9 25.1 %all_to_all.32.parts_ref = bf16[4,3072,128]{2,1,0:T(8,128)(2,1)S(1)} all-to-all(bf16[4,3072,128]{2,1,0:T(8,128)(2,1)S(1)} %bitcast.16), channel_id=1, replica_groups={{0,1,4,5},{2,3,6,7},{8,9,12,13},{10,11,14,15},{21,22,25,26},{23,20,27,2..., dimensions={0} | all-to-all | bytes 6291456 | tf_op jit(solution)/shard_map/all_to_all | solution.py:178
  104.9 0.4 shard_map.171
  105.3 10.1 %all_to_all.33.parts_ref = bf16[4,768,128]{2,1,0:T(8,128)(2,1)S(1)} all-to-all(bf16[4,768,128]{2,1,0:T(8,128)(2,1)S(1)} %bitcast.17), channel_id=1, replica_groups={{5,6,9,10},{7,4,11,8},{13,14,1,2},{15,12,3,0},{16,17,20,21},{18,19,22,2..., dimensions={0} | all-to-all | bytes 1572864 | tf_op jit(solution)/shard_map/all_to_all | solution.py:178
  115.4 0.1 shard_map.172
  115.5 26.8 %all_to_all.34 = bf16[32,24,128]{2,1,0:T(8,128)(2,1)S(1)} all-to-all(bf16[32,24,128]{2,1,0:T(8,128)(2,1)S(1)} %bitcast.20), channel_id=1, replica_groups=mesh['ep'=32,'tp'=16] {'ep'}, dimensions={0} | all-to-all | bytes 393216 | tf_op jit(solution)/shard_map/all_to_all | solution.py:178
  142.3 1.2 shard_map.173
Async XLA Ops:
  3.2 35.5 %all-to-all-start = ((bf16[32,24,128]{2,1,0:T(8,128)(2,1)}), bf16[32,24,128]{2,1,0:T(8,128)(2,1)S(1)}, u32[]{:S(2)}, u32[]{:S(2)}) async-start(bf16[32,24,128]{2,1,0:T(8,128)(2,1)} %bitcast.3), calls=%async_computation | async-start | bytes 393216 | tf_op jit(solution)/shard_map/all_to_all | solution.py:178
  22.1 4.3 %collective-permute-start = (bf16[32,128]{1,0:T(8,128)(2,1)S(1)}, bf16[32,128]{1,0:T(8,128)(2,1)S(1)}, u32[]{:S(2)}, u32[]{:S(2)}) collective-permute-start(bf16[32,128]{1,0:T(8,128)(2,1)S(1)} %get-tuple-element.9.gated_ref), channel_id=1, source_target_pairs={{0,16},{16,32},{32,48},{48,64},{64,80},{80,96},{96,112},{112,128},... | collective-permute-start | bytes 24584 | tf_op jit(solution)/shard_map/ppermute | solution.py:247
  51.0 25.2 %copy-start = (bf16[1,2048,256]{2,1,0:T(8,128)(2,1)S(1)}, bf16[1,2048,256]{2,1,0:T(8,128)(2,1)}, u32[]{:S(2)}) copy-start(bf16[1,2048,256]{2,1,0:T(8,128)(2,1)} %refs_1_.1) | copy-start | bytes 3145732
  51.0 25.2 %copy-start.1 = (bf16[1,2048,256]{2,1,0:T(8,128)(2,1)S(1)}, bf16[1,2048,256]{2,1,0:T(8,128)(2,1)}, u32[]{:S(2)}) copy-start(bf16[1,2048,256]{2,1,0:T(8,128)(2,1)} %refs_2_.1) | copy-start | bytes 3145732
  51.0 25.2 %copy-start.2 = (bf16[1,256,2048]{2,1,0:T(8,128)(2,1)S(1)}, bf16[1,256,2048]{2,1,0:T(8,128)(2,1)}, u32[]{:S(2)}) copy-start(bf16[1,256,2048]{2,1,0:T(8,128)(2,1)} %refs_3_.5) | copy-start | bytes 3145732
  51.0 25.2 %copy-start.3 = (bf16[512,128]{1,0:T(8,128)(2,1)S(1)}, bf16[512,128]{1,0:T(8,128)(2,1)}, u32[]{:S(2)}) copy-start(bf16[512,128]{1,0:T(8,128)(2,1)} %refs_6_.1) | copy-start | bytes 393220
  51.0 25.2 %copy-start.4 = (f32[512]{0:T(512)S(1)}, f32[512]{0:T(512)}, u32[]{:S(2)}) copy-start(f32[512]{0:T(512)} %param.22) | copy-start | bytes 6148
  51.1 25.2 %copy-start.5 = (f32[512]{0:T(512)S(1)}, f32[512]{0:T(512)}, u32[]{:S(2)}) copy-start(f32[512]{0:T(512)} %param.23) | copy-start | bytes 6148

commit v4 on v2

v4 whole, which is shorter than its diff:
```python
import math

import jax
import jax.numpy as jnp
from jax import lax
from jax.experimental import pallas as pl
from jax.experimental.pallas import tpu as pltpu
from jax.sharding import PartitionSpec as P


norm_eps = 1e-06
F32 = jnp.float32
BF16 = jnp.bfloat16


def call(body, outs, *operands, far=0):
    near = len(operands) - far
    operands = operands[:near] + tuple(pltpu.with_memory_space_constraint(x, pltpu.HBM) for x in operands[near:])

    def kernel(*refs):
        sources, results = refs[near : near + far], refs[near + far : near + far + len(outs)]
        if not far:
            body(*refs[:near], *results)
            return
        held, sems = refs[near + far + len(outs) : -1], refs[-1]
        copies = [pltpu.make_async_copy(sources[i], held[i], sems.at[i]) for i in range(far)]
        for copy in copies:
            copy.start()
        ready = set()

        def load(i):
            if i not in ready:
                copies[i].wait()
                ready.add(i)
            return held[i]

        body(load, *refs[:near], *results)

    scratch = [pltpu.VMEM(x.shape, x.dtype) for x in operands[near:]]
    return pl.pallas_call(
        kernel,
        out_shape=tuple(jax.ShapeDtypeStruct(s, d) for s, d in outs),
        in_specs=[pl.BlockSpec(memory_space=pltpu.VMEM)] * near + [pl.BlockSpec(memory_space=pltpu.HBM)] * far,
        out_specs=tuple([pl.BlockSpec(memory_space=pltpu.VMEM)] * len(outs)),
        scratch_shapes=scratch + [pltpu.SemaphoreType.DMA((far,))] * (far > 0),
        compiler_params=pltpu.CompilerParams(vmem_limit_bytes=20 * 1024 * 1024),
    )(*operands)


def column_of(row):
    size = row.shape[1]
    at = lax.broadcasted_iota(jnp.int32, (size, size), 0)
    to = lax.broadcasted_iota(jnp.int32, (size, size), 1)
    return jnp.sum(jnp.where(at == to, jnp.broadcast_to(row, (size, size)), 0.0), axis=1, keepdims=True)


def columns_of(row):
    return jnp.transpose(jnp.broadcast_to(row, (8, row.shape[1])))[:, 0:1]


def inv_rms(values):
    return lax.rsqrt(jnp.mean(values * values, axis=-1, keepdims=True) + norm_eps)


def dispatch(groups, capacity, width, load, out_ref, table_ref):
    routes = load(0)[...]
    logits = load(1)[...]
    rows_b = routes.shape[1]
    expert = lax.broadcasted_iota(jnp.int32, (groups, rows_b), 0)
    first = expert == routes[0:1, :]
    second = expert == routes[1:2, :]
    named = jnp.where(first | second, 1.0, 0.0)
    before = lax.broadcasted_iota(jnp.int32, (rows_b, rows_b), 0) < lax.broadcasted_iota(jnp.int32, (rows_b, rows_b), 1)
    earlier = jnp.dot(named.astype(BF16), jnp.where(before, 1.0, 0.0).astype(BF16), preferred_element_type=F32)
    slot = expert.astype(F32) * capacity + earlier
    slot_a = jnp.sum(jnp.where(first, slot, 0.0), axis=0, keepdims=True)
    slot_b = jnp.sum(jnp.where(second, slot, 0.0), axis=0, keepdims=True)
    gap = logits[0:1, :] - logits[1:2, :]
    table_ref[...] = jnp.concatenate([slot_a, slot_b, jax.nn.sigmoid(gap), jax.nn.sigmoid(-gap), jnp.zeros((4, rows_b), F32)], axis=0)
    code = jnp.where(first | second, earlier, -1.0)
    place = lax.broadcasted_iota(jnp.int32, (groups, capacity, rows_b), 1).astype(F32)
    chosen = jnp.where(code[:, None, :] == place, 1.0, 0.0).reshape(groups * capacity, rows_b).astype(BF16)
    gain_ref, rows_ref = load(2), load(3)
    scale = inv_rms(rows_ref[...].astype(F32))
    start = pl.multiple_of(lax.axis_index("tp") * width, width)
    share = rows_ref[:, pl.ds(start, width)].astype(F32)
    normed = (share * scale * gain_ref[:, pl.ds(start, width)]).astype(BF16)
    out_ref[...] = jnp.dot(chosen, normed, preferred_element_type=F32).astype(BF16)


def mixer_front(load, gated_ref, taps_ref):
    taps_ref[...] = jnp.concatenate([load(0)[...], column_of(load(1)[...])], axis=1)
    gain_ref = load(2)
    rows = load(3)[...].astype(F32)
    normed = (rows * inv_rms(rows) * gain_ref[...]).astype(BF16)
    nt = (((1,), (1,)), ((), ()))
    value = lax.dot_general(load(4)[...], normed, nt, preferred_element_type=F32)
    gate = lax.dot_general(load(5)[...], normed, nt, preferred_element_type=F32)
    gated_ref[...] = (value * jax.nn.sigmoid(gate)).astype(BF16)


def conv_and_copies(side, arrived_ref, prev_ref, gated_ref, taps_ref, out_ref):
    count, _, width = out_ref.shape
    half = arrived_ref.shape[0] // 2
    taps = taps_ref[...]
    reach = taps.shape[1] - 2
    both = jnp.concatenate([prev_ref[...].astype(F32), gated_ref[...].astype(F32)], axis=1)
    span = both.shape[1]
    total = taps[:, reach + 1 :] + taps[:, reach : reach + 1] * both[:, width:]
    for k in range(reach):
        moved = pltpu.roll(both, reach - k, 1)
        total = total + taps[:, k : k + 1] * moved[:, span - width :]
    conv_out = total.astype(BF16)
    odd = lax.axis_index("ep") % 2
    for p in range(2):
        start = pl.multiple_of((p + odd) % 2 * half, half)
        rows = arrived_ref[pl.ds(start, half), :]
        for j in range(count):
            if j % side % 2 == p:
                out_ref[j, :half, :] = rows
                out_ref[j, half:, :] = conv_out


def shard_part(rows, gate_ref, up_ref, down_ref):
    gate = jnp.dot(rows, gate_ref[0], preferred_element_type=F32)
    up = jnp.dot(rows, up_ref[0], preferred_element_type=F32)
    hidden = (gate * jax.nn.sigmoid(gate) * up).astype(BF16)
    return jnp.dot(hidden, down_ref[0], preferred_element_type=F32)


def own_shard(slots, x_ref, wg_ref, wu_ref, wd_ref, cgain_ref, cshift_ref, wo_ref, part_ref, mix_ref):
    count = x_ref.shape[0]
    rows = jnp.concatenate([x_ref[j, :slots, :] for j in range(count)], axis=1)
    part_ref[...] = shard_part(rows, wg_ref, wu_ref, wd_ref)
    values = jnp.concatenate([x_ref[j, slots:, :] for j in range(count)], axis=0).astype(F32)
    centered = values - jnp.mean(values, axis=0, keepdims=True)
    variance = jnp.mean(centered * centered, axis=0, keepdims=True)
    shaped = centered * lax.rsqrt(variance + norm_eps) * columns_of(cgain_ref[...]) + columns_of(cshift_ref[...])
    activated = (shaped * jax.nn.sigmoid(shaped)).astype(BF16)
    mix_ref[...] = lax.dot_general(activated, wo_ref[...], (((0,), (0,)), ((), ())), preferred_element_type=F32).astype(BF16)


def lent_shard(x_ref, part_ref, wg_ref, wu_ref, wd_ref, out_ref):
    count, slots, width = out_ref.shape
    rows = jnp.concatenate([x_ref[j, :slots, :] for j in range(count)], axis=1)
    total = (part_ref[...] + shard_part(rows, wg_ref, wu_ref, wd_ref)).astype(BF16)
    for j in range(count):
        out_ref[j] = total[:, j * width : (j + 1) * width]


def add_parts(side, parts_ref, out_ref):
    count, half, _ = parts_ref.shape
    odd = lax.axis_index("ep") % 2
    for p in range(2):
        total = None
        for j in range(count):
            if j % side % 2 == p:
                term = parts_ref[j].astype(F32)
                total = term if total is None else total + term
        start = pl.multiple_of((p + odd) % 2 * half, half)
        out_ref[pl.ds(start, half), :] = total.astype(BF16)


def combine(back_ref, table_ref, out_ref):
    rows_b = out_ref.shape[0]
    slots = back_ref.shape[0]
    table = jnp.transpose(table_ref[...])
    place = lax.broadcasted_iota(jnp.int32, (rows_b, slots), 1).astype(F32)
    back = back_ref[...]
    total = None
    for j in range(2):
        pick = jnp.where(table[:, j : j + 1] == place, 1.0, 0.0).astype(BF16)
        term = jnp.dot(pick, back, preferred_element_type=F32) * table[:, 2 + j : 3 + j]
        total = term if total is None else total + term
    out_ref[...] = total.astype(BF16)


def exchange(blocks, axis):
    return lax.all_to_all(blocks, axis, split_axis=0, concat_axis=0, tiled=True)


def neighbours(groups, side):
    pairs = []
    for e in range(groups):
        shift = e % 2
        for y in range(side):
            for x in range(side):
                pairs.append(((e * side + y) * side + x, (e * side + y) * side + (((x - shift) % side ^ 1) + shift) % side))
    return pairs


def on_device(
    mixer_input,
    mixer_gain,
    glu_value_weight,
    glu_gate_weight,
    conv_taps,
    conv_bias,
    channel_gain,
    channel_shift,
    mixer_out_weight,
    expert_input,
    expert_gain,
    routes,
    route_logits,
    gate_weight,
    up_weight,
    down_weight,
):
    groups = lax.axis_size("ep")
    parts = lax.axis_size("tp")
    rows_b, features = expert_input.shape
    width = features // parts
    capacity = 3 * rows_b // groups
    slots = groups * capacity
    channels, tokens = glu_value_weight.shape[0], mixer_input.shape[0]

    side = math.isqrt(parts)
    half = slots // 2
    pairs = neighbours(groups, side)
    shards = (gate_weight, up_weight, down_weight)
    lent = []
    for w in shards:
        lent.append(lax.ppermute(w, ("ep", "tp"), pairs))

    def front(*refs):
        dispatch(groups, capacity, width, *refs)

    outgoing, table = call(
        front,
        [((slots, width), BF16), ((8, rows_b), F32)],
        routes.T,
        route_logits.T,
        expert_gain[None, :],
        expert_input,
        far=4,
    )
    gated, taps = call(
        mixer_front,
        [((channels, tokens), BF16), ((channels, conv_taps.shape[1] + 1), F32)],
        conv_taps,
        conv_bias[None, :],
        mixer_gain[None, :],
        mixer_input,
        glu_value_weight,
        glu_gate_weight,
        far=6,
    )
    before = lax.ppermute(gated, "ep", [(i, i + 1) for i in range(groups - 1)])
    arrived = exchange(outgoing.reshape(groups, capacity, width), "ep").reshape(slots, width)

    def spread(*refs):
        conv_and_copies(side, *refs)

    (copies,) = call(spread, [((parts, half + channels, width), BF16)], arrived, before, gated, taps)
    gathered = exchange(copies, "tp")

    def own(*refs):
        own_shard(half, *refs)

    part, mixed = call(
        own,
        [((half, features), F32), ((tokens, width), BF16)],
        gathered,
        *shards,
        channel_gain[None, :],
        channel_shift[None, :],
        mixer_out_weight,
    )
    (partial,) = call(lent_shard, [((parts, half, width), BF16)], gathered, part, *lent)

    def total(*refs):
        add_parts(side, *refs)

    (summed,) = call(total, [((slots, width), BF16)], exchange(partial, "tp"))
    returned = exchange(summed.reshape(groups, capacity, width), "ep").reshape(slots, width)
    (combined,) = call(combine, [((rows_b, width), BF16)], returned, table)
    return mixed, combined


def solution(mesh):
    in_specs = (
        P("ep", None),
        P(),
        P("tp", None),
        P("tp", None),
        P("tp", None),
        P("tp"),
        P(),
        P(),
        P(None, "tp"),
        P("ep", None),
        P(),
        P("ep", None),
        P("ep", None),
        P("ep", None, "tp"),
        P("ep", None, "tp"),
        P("ep", "tp", None),
    )
    out_specs = (P("ep", "tp"), P("ep", "tp"))

    return jax.shard_map(on_device, mesh=mesh, in_specs=in_specs, out_specs=out_specs, check_vma=False)
```

time: 146 us -> 162 us (1.11)
  blocking collectives: 101 us -> 53.7 us
  waiting for transfers between devices: 13.1 us -> 52.1 us
  starting transfers between devices: 20.3 us -> 38.2 us
  local copies, waits for them, and re-layouts: 0.46 us -> 3.68 us
  Pallas kernels: 10.4 us -> 13 us
    all_to_all x5 -> x2, blocking collectives: 101 us -> 53.7 us  [exchange(): return lax.all_to_all(blocks, axis, split_axis=0, concat_axis=0, tiled=True)]
    ppermute x0 -> x3, waiting for transfers between devices: none -> 27.7 us  [on_device(): lent.append(lax.ppermute(w, ('ep', 'tp'), pairs))]
    all_to_all x1 -> x2, waiting for transfers between devices: 12.3 us -> 23.6 us  [exchange(): return lax.all_to_all(blocks, axis, split_axis=0, concat_axis=0, tiled=True)]
    ppermute x0 -> x3, starting transfers between devices: none -> 11 us  [on_device(): lent.append(lax.ppermute(w, ('ep', 'tp'), pairs))]
    all_to_all x1 -> x2, starting transfers between devices: 16.7 us -> 23.6 us  [exchange(): return lax.all_to_all(blocks, axis, split_axis=0, concat_axis=0, tiled=True)]
    unnamed x12, local copies, waits for them, and re-layouts: 0.04 us -> 3.68 us
    pallas_call x7, Pallas kernels: 10.4 us -> 13 us  [call(): pl.pallas_call(kernel, out_shape=tuple((jax.ShapeDtypeStruct(s, d) for s,...]
  transfers between devices with their start and end apart: 2 -> 6, of which waited for: 2 -> 6; matrix products, arithmetic and copies ran while one was open for 0% -> 0% of each run, Pallas kernels for 1% -> 3%
where the time goes in v4:
time: 162 us; the launch traced here: 161 us
  blocking collectives  53.7 us (33%)
  waiting for transfers between devices  52.1 us (32%)
  starting transfers between devices  38.2 us (24%)
  Pallas kernels  13 us (8%)
  local copies, waits for them, and re-layouts  3.68 us (2%)
    all_to_all x2, blocking collectives, exchange(): return lax.all_to_all(blocks, axis, split_axis=0, concat_axis=0, tiled=True)  53.7 us
    ppermute x3, waiting for transfers between devices, on_device(): lent.append(lax.ppermute(w, ('ep', 'tp'), pairs))  27.7 us
    all_to_all x2, starting transfers between devices, exchange(): return lax.all_to_all(blocks, axis, split_axis=0, concat_axis=0, tiled=True)  23.6 us
    all_to_all x2, waiting for transfers between devices, exchange(): return lax.all_to_all(blocks, axis, split_axis=0, concat_axis=0, tiled=True)  23.6 us
    pallas_call x7, Pallas kernels, call(): pl.pallas_call(kernel, out_shape=tuple((jax.ShapeDtypeStruct(s, d) for s,...  13 us
    ppermute x3, starting transfers between devices, on_device(): lent.append(lax.ppermute(w, ('ep', 'tp'), pairs))  11 us
    unnamed x12, local copies, waits for them, and re-layouts  3.68 us
    ppermute x1, starting transfers between devices, on_device(): before = lax.ppermute(gated, 'ep', [(i, i + 1) for i in range(groups - 1)])  3.54 us
  transfers between devices with their start and end apart: 6, of which 6 were waited for; matrix products, arithmetic and copies ran while one was open for 0% of the time, Pallas kernels for 3%

profile of v4, /device:TPU:1, one launch (start us, length us, event | category | flops | bytes accessed | tf_op | source)
XLA Modules:
  0.0 161.3 jit_solution(6273625448616230220)
XLA Ops:
  0.6 2.5 %shard_map.167 = (bf16[768,128]{1,0:T(8,128)(2,1)}, f32[8,256]{1,0:T(8,128)S(1)}) custom-call(s32[2,256]{1,0:T(2,128)} %bitcast.18, f32[2,256]{1,0:T(2,128)} %bitcast.19, f32[1,2048]{1,0:T(1,128)} %bitcast.16, bf16[256,2048]{1,0:T(8,128)(2,1)} %refs_3_.3), custom_call_target="tpu_custom_call" | custom-call | tf_op jit(solution)/shard_map/pallas_call | solution.py:40
  3.2 16.7 %all-to-all-start = ((bf16[32,24,128]{2,1,0:T(8,128)(2,1)}), bf16[32,24,128]{2,1,0:T(8,128)(2,1)S(1)}, u32[]{:S(2)}, u32[]{:S(2)}) async-start(bf16[32,24,128]{2,1,0:T(8,128)(2,1)} %bitcast.3), calls=%async_computation | async-start | bytes 393216 | tf_op jit(solution)/shard_map/all_to_all | solution.py:179
  19.9 2.1 %shard_map.168 = (bf16[32,128]{1,0:T(8,128)(2,1)S(1)}, f32[32,32]{1,0:T(8,128)S(1)}) custom-call(f32[32,31]{1,0:T(8,128)} %refs_0_.1, f32[1,32]{1,0:T(1,128)} %bitcast.20, f32[1,2048]{1,0:T(1,128)} %bitcast.17, bf16[128,2048]{1,0:T(8,128)(2,1)} %refs_3_.4, bf16[32,2048]{1,0:T(8,128)(2,1)} %refs_4_.1, bf16[32,2048]{1,0:T(8,128)(2,1)} %refs_5_.1), custom_call_target="tpu_custom_call" | custom-call | tf_op jit(solution)/shard_map/pallas_call | solution.py:40
  22.1 3.5 %collective-permute-start = (bf16[32,128]{1,0:T(8,128)(2,1)S(1)}, bf16[32,128]{1,0:T(8,128)(2,1)S(1)}, u32[]{:S(2)}, u32[]{:S(2)}) collective-permute-start(bf16[32,128]{1,0:T(8,128)(2,1)S(1)} %get-tuple-element.9.refs_2_), channel_id=1, source_target_pairs={{0,16},{16,32},{32,48},{48,64},{64,80},{80,96},{96,112},{112,128},... | collective-permute-start | bytes 24584 | tf_op jit(solution)/shard_map/ppermute | solution.py:249
  25.6 0.8 collective-permute-done.refs_1_
  26.4 12.3 %all-to-all-done = bf16[32,24,128]{2,1,0:T(8,128)(2,1)S(1)} async-done(((bf16[32,24,128]{2,1,0:T(8,128)(2,1)}), bf16[32,24,128]{2,1,0:T(8,128)(2,1)S(1)}, u32[]{:S(2)}, u32[]{:S(2)}) %all-to-all-start) | async-done | bytes 196640 | tf_op jit(solution)/shard_map/all_to_all | solution.py:179
  38.7 1.8 %shard_map.169 = bf16[16,416,128]{2,1,0:T(8,128)(2,1)} custom-call(bf16[768,128]{1,0:T(8,128)(2,1)S(1)} %bitcast.11, bf16[32,128]{1,0:T(8,128)(2,1)S(1)} %collective-permute-done.refs_1_, bf16[32,128]{1,0:T(8,128)(2,1)S(1)} %get-tuple-element.9.refs_2_, f32[32,32]{1,0:T(8,128)S(1)} %get-tuple-element.10.refs_3_), custom_call_target="tpu_custom_call" | custom-call | tf_op jit(solution)/shard_map/pallas_call | solution.py:40
  40.5 0.0 copy-start.3
  40.5 0.0 copy-start.4
  40.5 0.0 copy-start.5
  40.5 6.9 %all-to-all-start.1 = ((bf16[16,416,128]{2,1,0:T(8,128)(2,1)}), bf16[16,416,128]{2,1,0:T(8,128)(2,1)S(1)}, u32[]{:S(2)}, u32[]{:S(2)}) async-start(bf16[16,416,128]{2,1,0:T(8,128)(2,1)} %shard_map.169), calls=%async_computation.1 | async-start | bytes 3407872 | tf_op jit(solution)/shard_map/all_to_all | solution.py:179
  47.4 4.5 %collective-permute-start.1 = (bf16[1,2048,256]{2,1,0:T(8,128)(2,1)}, bf16[1,2048,256]{2,1,0:T(8,128)(2,1)S(1)}, u32[]{:S(2)}, u32[]{:S(2)}) collective-permute-start(bf16[1,2048,256]{2,1,0:T(8,128)(2,1)} %refs_1_.1), channel_id=1, source_target_pairs={{0,1},{1,0},{2,3},{3,2},{4,5},{5,4},{6,7},{7,6},{8,9},{9,8},{10,11... | collective-permute-start | bytes 3145736 | tf_op jit(solution)/shard_map/ppermute | solution.py:224
  51.9 2.0 %collective-permute-start.2 = (bf16[1,2048,256]{2,1,0:T(8,128)(2,1)}, bf16[1,2048,256]{2,1,0:T(8,128)(2,1)}, u32[]{:S(2)}, u32[]{:S(2)}) collective-permute-start(bf16[1,2048,256]{2,1,0:T(8,128)(2,1)} %refs_2_.1), channel_id=1, source_target_pairs={{0,1},{1,0},{2,3},{3,2},{4,5},{5,4},{6,7},{7,6},{8,9},{9,8},{10,11... | collective-permute-start | bytes 3145736 | tf_op jit(solution)/shard_map/ppermute | solution.py:224
  53.9 4.5 %collective-permute-start.3 = (bf16[1,256,2048]{2,1,0:T(8,128)(2,1)}, bf16[1,256,2048]{2,1,0:T(8,128)(2,1)}, u32[]{:S(2)}, u32[]{:S(2)}) collective-permute-start(bf16[1,256,2048]{2,1,0:T(8,128)(2,1)} %refs_3_.5), channel_id=1, source_target_pairs={{0,1},{1,0},{2,3},{3,2},{4,5},{5,4},{6,7},{7,6},{8,9},{9,8},{10,11... | collective-permute-start | bytes 3145736 | tf_op jit(solution)/shard_map/ppermute | solution.py:224
  58.4 11.3 %all-to-all-done.1.refs_0_ = bf16[16,416,128]{2,1,0:T(8,128)(2,1)S(1)} async-done(((bf16[16,416,128]{2,1,0:T(8,128)(2,1)}), bf16[16,416,128]{2,1,0:T(8,128)(2,1)S(1)}, u32[]{:S(2)}, u32[]{:S(2)}) %all-to-all-start.1) | async-done | bytes 1703968 | tf_op jit(solution)/shard_map/all_to_all | solution.py:179
  69.7 0.0 copy-done.3
  69.7 0.0 copy-done.4
  69.7 0.0 copy-done.5
  69.7 0.0 copy-start
  69.7 1.2 copy-done
  70.9 0.0 copy-start.1
  70.9 1.2 copy-done.1
  72.1 1.2 copy-done.2
  73.3 2.1 %shard_map.170 = (f32[384,2048]{1,0:T(8,128)S(1)}, bf16[128,128]{1,0:T(8,128)(2,1)}) custom-call(bf16[16,416,128]{2,1,0:T(8,128)(2,1)S(1)} %all-to-all-done.1.refs_0_, bf16[1,2048,256]{2,1,0:T(8,128)(2,1)S(1)} %copy-done, bf16[1,2048,256]{2,1,0:T(8,128)(2,1)S(1)} %copy-done.1, bf16[1,256,2048]{2,1,0:T(8,128)(2,1)S(1)} %copy-done.2, f32[1,512]{1,0:T(1,128)S(1)} %bitcast.14, ...), custom_call_target="tpu_custom_call" | custom-call | tf_op jit(solution)/shard_map/pallas_call | solution.py:40
  75.5 5.1 %collective-permute-done.1.refs_2_ = bf16[1,2048,256]{2,1,0:T(8,128)(2,1)S(1)} collective-permute-done((bf16[1,2048,256]{2,1,0:T(8,128)(2,1)}, bf16[1,2048,256]{2,1,0:T(8,128)(2,1)S(1)}, u32[]{:S(2)}, u32[]{:S(2)}) %collective-permute-start.1) | collective-permute-done | bytes 1048608 | tf_op jit(solution)/shard_map/ppermute | solution.py:224
  80.6 11.3 %collective-permute-done.2.refs_3_ = bf16[1,2048,256]{2,1,0:T(8,128)(2,1)} collective-permute-done((bf16[1,2048,256]{2,1,0:T(8,128)(2,1)}, bf16[1,2048,256]{2,1,0:T(8,128)(2,1)}, u32[]{:S(2)}, u32[]{:S(2)}) %collective-permute-start.2) | collective-permute-done | bytes 1048608 | tf_op jit(solution)/shard_map/ppermute | solution.py:224
  91.9 11.2 %collective-permute-done.3.refs_4_ = bf16[1,256,2048]{2,1,0:T(8,128)(2,1)} collective-permute-done((bf16[1,256,2048]{2,1,0:T(8,128)(2,1)}, bf16[1,256,2048]{2,1,0:T(8,128)(2,1)}, u32[]{:S(2)}, u32[]{:S(2)}) %collective-permute-start.3) | collective-permute-done | bytes 1048608 | tf_op jit(solution)/shard_map/ppermute | solution.py:224
  103.2 3.0 %shard_map.171 = bf16[16,384,128]{2,1,0:T(8,128)(2,1)S(1)} custom-call(bf16[16,416,128]{2,1,0:T(8,128)(2,1)S(1)} %all-to-all-done.1.refs_0_, f32[384,2048]{1,0:T(8,128)S(1)} %get-tuple-element.12.refs_1_, bf16[1,2048,256]{2,1,0:T(8,128)(2,1)S(1)} %collective-permute-done.1.refs_2_, bf16[1,2048,256]{2,1,0:T(8,128)(2,1)} %collective-permute-done.2.refs_3_, ...), custom_call_target="tpu_custom_call" | custom-call | tf_op jit(solution)/shard_map/pallas_call | solution.py:40
  106.2 29.0 %all_to_all.20.refs_0_ = bf16[16,384,128]{2,1,0:T(8,128)(2,1)S(1)} all-to-all(bf16[16,384,128]{2,1,0:T(8,128)(2,1)S(1)} %shard_map.171), channel_id=1, replica_groups=mesh['ep'=32,'tp'=16] {'tp'}, dimensions={0} | all-to-all | bytes 3145728 | tf_op jit(solution)/shard_map/all_to_all | solution.py:179
  135.1 0.2 shard_map.172
  135.3 24.7 %all_to_all.21 = bf16[32,24,128]{2,1,0:T(8,128)(2,1)S(1)} all-to-all(bf16[32,24,128]{2,1,0:T(8,128)(2,1)S(1)} %bitcast.12), channel_id=1, replica_groups=mesh['ep'=32,'tp'=16] {'ep'}, dimensions={0} | all-to-all | bytes 393216 | tf_op jit(solution)/shard_map/all_to_all | solution.py:179
  160.1 1.2 shard_map.173
  (1 shorter events, 0.0 us)
Async XLA Ops:
  3.2 35.5 %all-to-all-start = ((bf16[32,24,128]{2,1,0:T(8,128)(2,1)}), bf16[32,24,128]{2,1,0:T(8,128)(2,1)S(1)}, u32[]{:S(2)}, u32[]{:S(2)}) async-start(bf16[32,24,128]{2,1,0:T(8,128)(2,1)} %bitcast.3), calls=%async_computation | async-start | bytes 393216 | tf_op jit(solution)/shard_map/all_to_all | solution.py:179
  22.1 4.3 %collective-permute-start = (bf16[32,128]{1,0:T(8,128)(2,1)S(1)}, bf16[32,128]{1,0:T(8,128)(2,1)S(1)}, u32[]{:S(2)}, u32[]{:S(2)}) collective-permute-start(bf16[32,128]{1,0:T(8,128)(2,1)S(1)} %get-tuple-element.9.refs_2_), channel_id=1, source_target_pairs={{0,16},{16,32},{32,48},{48,64},{64,80},{80,96},{96,112},{112,128},... | collective-permute-start | bytes 24584 | tf_op jit(solution)/shard_map/ppermute | solution.py:249
  40.5 29.2 %copy-start.3 = (bf16[512,128]{1,0:T(8,128)(2,1)S(1)}, bf16[512,128]{1,0:T(8,128)(2,1)}, u32[]{:S(2)}) copy-start(bf16[512,128]{1,0:T(8,128)(2,1)} %refs_6_.1) | copy-start | bytes 393220
  40.5 29.2 %copy-start.4 = (f32[512]{0:T(512)S(1)}, f32[512]{0:T(512)}, u32[]{:S(2)}) copy-start(f32[512]{0:T(512)} %param.22) | copy-start | bytes 6148
  40.5 29.2 %copy-start.5 = (f32[512]{0:T(512)S(1)}, f32[512]{0:T(512)}, u32[]{:S(2)}) copy-start(f32[512]{0:T(512)} %param.23) | copy-start | bytes 6148
  40.5 29.2 %all-to-all-start.1 = ((bf16[16,416,128]{2,1,0:T(8,128)(2,1)}), bf16[16,416,128]{2,1,0:T(8,128)(2,1)S(1)}, u32[]{:S(2)}, u32[]{:S(2)}) async-start(bf16[16,416,128]{2,1,0:T(8,128)(2,1)} %shard_map.169), calls=%async_computation.1 | async-start | bytes 3407872 | tf_op jit(solution)/shard_map/all_to_all | solution.py:179
  47.4 33.2 %collective-permute-start.1 = (bf16[1,2048,256]{2,1,0:T(8,128)(2,1)}, bf16[1,2048,256]{2,1,0:T(8,128)(2,1)S(1)}, u32[]{:S(2)}, u32[]{:S(2)}) collective-permute-start(bf16[1,2048,256]{2,1,0:T(8,128)(2,1)} %refs_1_.1), channel_id=1, source_target_pairs={{0,1},{1,0},{2,3},{3,2},{4,5},{5,4},{6,7},{7,6},{8,9},{9,8},{10,11... | collective-permute-start | bytes 3145736 | tf_op jit(solution)/shard_map/ppermute | solution.py:224
  51.9 40.1 %collective-permute-start.2 = (bf16[1,2048,256]{2,1,0:T(8,128)(2,1)}, bf16[1,2048,256]{2,1,0:T(8,128)(2,1)}, u32[]{:S(2)}, u32[]{:S(2)}) collective-permute-start(bf16[1,2048,256]{2,1,0:T(8,128)(2,1)} %refs_2_.1), channel_id=1, source_target_pairs={{0,1},{1,0},{2,3},{3,2},{4,5},{5,4},{6,7},{7,6},{8,9},{9,8},{10,11... | collective-permute-start | bytes 3145736 | tf_op jit(solution)/shard_map/ppermute | solution.py:224
  53.9 49.3 %collective-permute-start.3 = (bf16[1,256,2048]{2,1,0:T(8,128)(2,1)}, bf16[1,256,2048]{2,1,0:T(8,128)(2,1)}, u32[]{:S(2)}, u32[]{:S(2)}) collective-permute-start(bf16[1,256,2048]{2,1,0:T(8,128)(2,1)} %refs_3_.5), channel_id=1, source_target_pairs={{0,1},{1,0},{2,3},{3,2},{4,5},{5,4},{6,7},{7,6},{8,9},{9,8},{10,11... | collective-permute-start | bytes 3145736 | tf_op jit(solution)/shard_map/ppermute | solution.py:224
  69.7 1.2 copy-start
  70.9 1.2 copy-start.1
  72.1 1.2 copy-start.2

commit v5 on v4

--- a/solution.py
+++ b/solution.py
@@ -99,9 +99,19 @@
     gated_ref[...] = (value * jax.nn.sigmoid(gate)).astype(BF16)
 
 
-def conv_and_copies(side, arrived_ref, prev_ref, gated_ref, taps_ref, out_ref):
-    count, _, width = out_ref.shape
-    half = arrived_ref.shape[0] // 2
+def row_class(j, side):
+    return (j // side + j % side) % 2
+
+
+def spread_rows(side, arrived_ref, out_ref):
+    half = out_ref.shape[1]
+    for j in range(out_ref.shape[0]):
+        p = row_class(j, side)
+        out_ref[j] = arrived_ref[p * half : (p + 1) * half, :]
+
+
+def convolved(prev_ref, gated_ref, taps_ref):
+    width = gated_ref.shape[1]
     taps = taps_ref[...]
     reach = taps.shape[1] - 2
     both = jnp.concatenate([prev_ref[...].astype(F32), gated_ref[...].astype(F32)], axis=1)
@@ -110,15 +120,7 @@
     for k in range(reach):
         moved = pltpu.roll(both, reach - k, 1)
         total = total + taps[:, k : k + 1] * moved[:, span - width :]
-    conv_out = total.astype(BF16)
-    odd = lax.axis_index("ep") % 2
-    for p in range(2):
-        start = pl.multiple_of((p + odd) % 2 * half, half)
-        rows = arrived_ref[pl.ds(start, half), :]
-        for j in range(count):
-            if j % side % 2 == p:
-                out_ref[j, :half, :] = rows
-                out_ref[j, half:, :] = conv_out
+    return total.astype(BF16)
 
 
 def shard_part(rows, gate_ref, up_ref, down_ref):
@@ -128,37 +130,40 @@
     return jnp.dot(hidden, down_ref[0], preferred_element_type=F32)
 
 
-def own_shard(slots, x_ref, wg_ref, wu_ref, wd_ref, cgain_ref, cshift_ref, wo_ref, part_ref, mix_ref):
-    count = x_ref.shape[0]
-    rows = jnp.concatenate([x_ref[j, :slots, :] for j in range(count)], axis=1)
+def own_shard(x_ref, wg_ref, wu_ref, wd_ref, part_ref):
+    rows = jnp.concatenate([x_ref[j] for j in range(x_ref.shape[0])], axis=1)
     part_ref[...] = shard_part(rows, wg_ref, wu_ref, wd_ref)
-    values = jnp.concatenate([x_ref[j, slots:, :] for j in range(count)], axis=0).astype(F32)
+
+
+def lent_shard(x_ref, part_ref, wg_ref, wu_ref, wd_ref, prev_ref, gated_ref, taps_ref, out_ref):
+    count, slots, width = x_ref.shape
+    conv_out = convolved(prev_ref, gated_ref, taps_ref)
+    for j in range(count):
+        out_ref[j, slots:, :] = conv_out
+    rows = jnp.concatenate([x_ref[j] for j in range(count)], axis=1)
+    total = (part_ref[...] + shard_part(rows, wg_ref, wu_ref, wd_ref)).astype(BF16)
+    for j in range(count):
+        out_ref[j, :slots, :] = total[:, j * width : (j + 1) * width]
+
+
+def mixer_tail(slots, parts_ref, cgain_ref, cshift_ref, wo_ref, out_ref):
+    values = jnp.concatenate([parts_ref[j, slots:, :] for j in range(parts_ref.shape[0])], axis=0).astype(F32)
     centered = values - jnp.mean(values, axis=0, keepdims=True)
     variance = jnp.mean(centered * centered, axis=0, keepdims=True)
     shaped = centered * lax.rsqrt(variance + norm_eps) * columns_of(cgain_ref[...]) + columns_of(cshift_ref[...])
     activated = (shaped * jax.nn.sigmoid(shaped)).astype(BF16)
-    mix_ref[...] = lax.dot_general(activated, wo_ref[...], (((0,), (0,)), ((), ())), preferred_element_type=F32).astype(BF16)
-
-
-def lent_shard(x_ref, part_ref, wg_ref, wu_ref, wd_ref, out_ref):
-    count, slots, width = out_ref.shape
-    rows = jnp.concatenate([x_ref[j, :slots, :] for j in range(count)], axis=1)
-    total = (part_ref[...] + shard_part(rows, wg_ref, wu_ref, wd_ref)).astype(BF16)
-    for j in range(count):
-        out_ref[j] = total[:, j * width : (j + 1) * width]
+    out_ref[...] = lax.dot_general(activated, wo_ref[...], (((0,), (0,)), ((), ())), preferred_element_type=F32).astype(BF16)
 
 
 def add_parts(side, parts_ref, out_ref):
-    count, half, _ = parts_ref.shape
-    odd = lax.axis_index("ep") % 2
+    count, half = parts_ref.shape[0], out_ref.shape[0] // 2
     for p in range(2):
         total = None
         for j in range(count):
-            if j % side % 2 == p:
-                term = parts_ref[j].astype(F32)
+            if row_class(j, side) == p:
+                term = parts_ref[j, :half, :].astype(F32)
                 total = term if total is None else total + term
-        start = pl.multiple_of((p + odd) % 2 * half, half)
-        out_ref[pl.ds(start, half), :] = total.astype(BF16)
+        out_ref[p * half : (p + 1) * half, :] = total.astype(BF16)
 
 
 def combine(back_ref, table_ref, out_ref):
@@ -179,13 +184,18 @@
     return lax.all_to_all(blocks, axis, split_axis=0, concat_axis=0, tiled=True)
 
 
-def neighbours(groups, side):
+def neighbours(groups, side, along_x):
     pairs = []
     for e in range(groups):
         shift = e % 2
+
+        def other(at):
+            return (((at - shift) % side ^ 1) + shift) % side
+
         for y in range(side):
             for x in range(side):
-                pairs.append(((e * side + y) * side + x, (e * side + y) * side + (((x - shift) % side ^ 1) + shift) % side))
+                to = (y, other(x)) if along_x else (other(y), x)
+                pairs.append(((e * side + y) * side + x, (e * side + to[0]) * side + to[1]))
     return pairs
 
 
@@ -217,11 +227,8 @@
 
     side = math.isqrt(parts)
     half = slots // 2
-    pairs = neighbours(groups, side)
     shards = (gate_weight, up_weight, down_weight)
-    lent = []
-    for w in shards:
-        lent.append(lax.ppermute(w, ("ep", "tp"), pairs))
+
 
     def front(*refs):
         dispatch(groups, capacity, width, *refs)
@@ -247,32 +254,28 @@
         far=6,
     )
     before = lax.ppermute(gated, "ep", [(i, i + 1) for i in range(groups - 1)])
+    lent = []
+    for w in shards:
+        lent.append(lax.ppermute(w, ("ep", "tp"), neighbours(groups, side, True)))
     arrived = exchange(outgoing.reshape(groups, capacity, width), "ep").reshape(slots, width)
 
     def spread(*refs):
-        conv_and_copies(side, *refs)
-
-    (copies,) = call(spread, [((parts, half + channels, width), BF16)], arrived, before, gated, taps)
+        spread_rows(side, *refs)
+
+    (copies,) = call(spread, [((parts, half, width), BF16)], arrived)
     gathered = exchange(copies, "tp")
-
-    def own(*refs):
-        own_shard(half, *refs)
-
-    part, mixed = call(
-        own,
-        [((half, features), F32), ((tokens, width), BF16)],
-        gathered,
-        *shards,
-        channel_gain[None, :],
-        channel_shift[None, :],
-        mixer_out_weight,
-    )
-    (partial,) = call(lent_shard, [((parts, half, width), BF16)], gathered, part, *lent)
+    (part,) = call(own_shard, [((half, features), F32)], gathered, *shards)
+    (partial,) = call(lent_shard, [((parts, half + channels, width), BF16)], gathered, part, *lent, before, gated, taps)
+    partials = exchange(partial, "tp")
 
     def total(*refs):
         add_parts(side, *refs)
 
-    (summed,) = call(total, [((slots, width), BF16)], exchange(partial, "tp"))
+    def tail(*refs):
+        mixer_tail(half, *refs)
+
+    (summed,) = call(total, [((slots, width), BF16)], partials)
+    (mixed,) = call(tail, [((tokens, width), BF16)], partials, channel_gain[None, :], channel_shift[None, :], mixer_out_weight)
     returned = exchange(summed.reshape(groups, capacity, width), "ep").reshape(slots, width)
     (combined,) = call(combine, [((rows_b, width), BF16)], returned, table)
     return mixed, combined

time: 162 us -> 161 us (level)
  starting transfers between devices: 38.2 us -> 25.6 us
  blocking collectives: 53.7 us -> 65.8 us
    all_to_all x2, blocking collectives: 53.7 us -> 65.8 us  [exchange(): return lax.all_to_all(blocks, axis, split_axis=0, concat_axis=0, tiled=True)]
    all_to_all x2, starting transfers between devices: 23.6 us -> 12.6 us  [exchange(): return lax.all_to_all(blocks, axis, split_axis=0, concat_axis=0, tiled=True)]
    ppermute x3, waiting for transfers between devices: 27.7 us -> 29.6 us  [on_device(): lent.append(lax.ppermute(w, ('ep', 'tp'), neighbours(groups, side, True)))]
    pallas_call x7 -> x8, Pallas kernels: 13 us -> 13.5 us  [call(): pl.pallas_call(kernel, out_shape=tuple((jax.ShapeDtypeStruct(s, d) for s,...]
  transfers between devices with their start and end apart: 6 -> 6, of which waited for: 6 -> 5; matrix products, arithmetic and copies ran while one was open for 0% -> 0% of each run, Pallas kernels for 3% -> 3%
where the time goes in v5:
time: 161 us
  blocking collectives  65.8 us (41%)
  waiting for transfers between devices  52.8 us (33%)
  starting transfers between devices  25.6 us (16%)
  Pallas kernels  13.5 us (8%)
  local copies, waits for them, and re-layouts  2.46 us (2%)
    all_to_all x2, blocking collectives, exchange(): return lax.all_to_all(blocks, axis, split_axis=0, concat_axis=0, tiled=True)  65.8 us
    ppermute x3, waiting for transfers between devices, on_device(): lent.append(lax.ppermute(w, ('ep', 'tp'), neighbours(groups, side, True)))  29.6 us
    all_to_all x2, waiting for transfers between devices, exchange(): return lax.all_to_all(blocks, axis, split_axis=0, concat_axis=0, tiled=True)  23.2 us
    pallas_call x8, Pallas kernels, call(): pl.pallas_call(kernel, out_shape=tuple((jax.ShapeDtypeStruct(s, d) for s,...  13.5 us
    all_to_all x2, starting transfers between devices, exchange(): return lax.all_to_all(blocks, axis, split_axis=0, concat_axis=0, tiled=True)  12.6 us
    ppermute x3, starting transfers between devices, on_device(): lent.append(lax.ppermute(w, ('ep', 'tp'), neighbours(groups, side, True)))  11 us
  transfers between devices with their start and end apart: 6, of which 5 were waited for; matrix products, arithmetic and copies ran while one was open for 0% of the time, Pallas kernels for 3%

profile of v5, /device:TPU:1, one launch (start us, length us, event | category | flops | bytes accessed | tf_op | source)
XLA Modules:
  0.0 160.8 jit_solution(5929463675421362853)
XLA Ops:
  0.6 1.9 %shard_map.167 = (bf16[768,128]{1,0:T(8,128)(2,1)S(1)}, f32[8,256]{1,0:T(8,128)S(1)}) custom-call(s32[2,256]{1,0:T(2,128)} %bitcast.18, f32[2,256]{1,0:T(2,128)} %bitcast.19, f32[1,2048]{1,0:T(1,128)} %bitcast.16, bf16[256,2048]{1,0:T(8,128)(2,1)} %refs_3_.4), custom_call_target="tpu_custom_call" | custom-call | tf_op jit(solution)/shard_map/pallas_call | solution.py:40
  2.5 35.3 %all_to_all.20 = bf16[32,24,128]{2,1,0:T(8,128)(2,1)S(1)} all-to-all(bf16[32,24,128]{2,1,0:T(8,128)(2,1)S(1)} %bitcast.13), channel_id=1, replica_groups=mesh['ep'=32,'tp'=16] {'ep'}, dimensions={0} | all-to-all | bytes 393216 | tf_op jit(solution)/shard_map/all_to_all | solution.py:184
  37.8 1.4 shard_map.168
  39.2 0.0 copy-start
  39.2 6.9 %all-to-all-start.1 = ((bf16[16,384,128]{2,1,0:T(8,128)(2,1)}), bf16[16,384,128]{2,1,0:T(8,128)(2,1)S(1)}, u32[]{:S(2)}, u32[]{:S(2)}) async-start(bf16[16,384,128]{2,1,0:T(8,128)(2,1)} %shard_map.168), calls=%async_computation.1 | async-start | bytes 3145728 | tf_op jit(solution)/shard_map/all_to_all | solution.py:184
  46.1 0.0 copy-done
  46.1 4.5 %collective-permute-start = (bf16[1,2048,256]{2,1,0:T(8,128)(2,1)S(1)}, bf16[1,2048,256]{2,1,0:T(8,128)(2,1)}, u32[]{:S(2)}, u32[]{:S(2)}) collective-permute-start(bf16[1,2048,256]{2,1,0:T(8,128)(2,1)S(1)} %copy-done), channel_id=1, source_target_pairs={{0,1},{1,0},{2,3},{3,2},{4,5},{5,4},{6,7},{7,6},{8,9},{9,8},{10,11... | collective-permute-start | bytes 3145736 | tf_op jit(solution)/shard_map/ppermute | solution.py:259
  50.6 2.0 %collective-permute-start.1 = (bf16[1,2048,256]{2,1,0:T(8,128)(2,1)}, bf16[1,2048,256]{2,1,0:T(8,128)(2,1)}, u32[]{:S(2)}, u32[]{:S(2)}) collective-permute-start(bf16[1,2048,256]{2,1,0:T(8,128)(2,1)} %refs_2_.1), channel_id=1, source_target_pairs={{0,1},{1,0},{2,3},{3,2},{4,5},{5,4},{6,7},{7,6},{8,9},{9,8},{10,11... | collective-permute-start | bytes 3145736 | tf_op jit(solution)/shard_map/ppermute | solution.py:259
  52.6 4.5 %collective-permute-start.2 = (bf16[1,256,2048]{2,1,0:T(8,128)(2,1)}, bf16[1,256,2048]{2,1,0:T(8,128)(2,1)}, u32[]{:S(2)}, u32[]{:S(2)}) collective-permute-start(bf16[1,256,2048]{2,1,0:T(8,128)(2,1)} %refs_3_.5), channel_id=1, source_target_pairs={{0,1},{1,0},{2,3},{3,2},{4,5},{5,4},{6,7},{7,6},{8,9},{9,8},{10,11... | collective-permute-start | bytes 3145736 | tf_op jit(solution)/shard_map/ppermute | solution.py:259
  57.1 2.1 %shard_map.170 = (bf16[32,128]{1,0:T(8,128)(2,1)S(1)}, f32[32,32]{1,0:T(8,128)S(1)}) custom-call(f32[32,31]{1,0:T(8,128)} %refs_0_.1, f32[1,32]{1,0:T(1,128)} %bitcast.20, f32[1,2048]{1,0:T(1,128)} %bitcast.17, bf16[128,2048]{1,0:T(8,128)(2,1)} %refs_3_.6, bf16[32,2048]{1,0:T(8,128)(2,1)} %refs_4_.1, bf16[32,2048]{1,0:T(8,128)(2,1)} %refs_5_.1), custom_call_target="tpu_custom_call" | custom-call | tf_op jit(solution)/shard_map/pallas_call | solution.py:40
  59.3 2.0 %collective-permute-start.3 = (bf16[32,128]{1,0:T(8,128)(2,1)S(1)}, bf16[32,128]{1,0:T(8,128)(2,1)S(1)}, u32[]{:S(2)}, u32[]{:S(2)}) collective-permute-start(bf16[32,128]{1,0:T(8,128)(2,1)S(1)} %get-tuple-element.7.refs_6_), channel_id=1, source_target_pairs={{0,16},{16,32},{32,48},{48,64},{64,80},{80,96},{96,112},{112,128},... | collective-permute-start | bytes 24584 | tf_op jit(solution)/shard_map/ppermute | solution.py:256
  61.3 5.7 %all-to-all-done.1.refs_0_ = bf16[16,384,128]{2,1,0:T(8,128)(2,1)S(1)} async-done(((bf16[16,384,128]{2,1,0:T(8,128)(2,1)}), bf16[16,384,128]{2,1,0:T(8,128)(2,1)S(1)}, u32[]{:S(2)}, u32[]{:S(2)}) %all-to-all-start.1) | async-done | bytes 1572896 | tf_op jit(solution)/shard_map/all_to_all | solution.py:184
  67.0 0.0 copy-start.1
  67.0 1.2 copy-done.1
  68.2 0.0 copy-start.2
  68.2 1.2 copy-done.2
  69.4 1.4 shard_map.169.refs_1_
  70.9 0.0 collective-permute-done.3.refs_5_
  70.9 7.1 %collective-permute-done.refs_2_ = bf16[1,2048,256]{2,1,0:T(8,128)(2,1)} collective-permute-done((bf16[1,2048,256]{2,1,0:T(8,128)(2,1)S(1)}, bf16[1,2048,256]{2,1,0:T(8,128)(2,1)}, u32[]{:S(2)}, u32[]{:S(2)}) %collective-permute-start) | collective-permute-done | bytes 1048608 | tf_op jit(solution)/shard_map/ppermute | solution.py:259
  78.0 11.2 %collective-permute-done.1.refs_3_ = bf16[1,2048,256]{2,1,0:T(8,128)(2,1)} collective-permute-done((bf16[1,2048,256]{2,1,0:T(8,128)(2,1)}, bf16[1,2048,256]{2,1,0:T(8,128)(2,1)}, u32[]{:S(2)}, u32[]{:S(2)}) %collective-permute-start.1) | collective-permute-done | bytes 1048608 | tf_op jit(solution)/shard_map/ppermute | solution.py:259
  89.2 11.2 %collective-permute-done.2.refs_4_ = bf16[1,256,2048]{2,1,0:T(8,128)(2,1)} collective-permute-done((bf16[1,256,2048]{2,1,0:T(8,128)(2,1)}, bf16[1,256,2048]{2,1,0:T(8,128)(2,1)}, u32[]{:S(2)}, u32[]{:S(2)}) %collective-permute-start.2) | collective-permute-done | bytes 1048608 | tf_op jit(solution)/shard_map/ppermute | solution.py:259
  100.5 3.4 %shard_map.171 = bf16[16,416,128]{2,1,0:T(8,128)(2,1)S(1)} custom-call(bf16[16,384,128]{2,1,0:T(8,128)(2,1)S(1)} %all-to-all-done.1.refs_0_, f32[384,2048]{1,0:T(8,128)S(1)} %shard_map.169.refs_1_, bf16[1,2048,256]{2,1,0:T(8,128)(2,1)} %collective-permute-done.refs_2_, bf16[1,2048,256]{2,1,0:T(8,128)(2,1)} %collective-permute-done.1.refs_3_, ...), custom_call_target="tpu_custom_call" | custom-call | tf_op jit(solution)/shard_map/pallas_call | solution.py:40
  103.8 30.4 %all_to_all.21.refs_0_ = bf16[16,416,128]{2,1,0:T(8,128)(2,1)S(1)} all-to-all(bf16[16,416,128]{2,1,0:T(8,128)(2,1)S(1)} %shard_map.171), channel_id=1, replica_groups=mesh['ep'=32,'tp'=16] {'tp'}, dimensions={0} | all-to-all | bytes 3407872 | tf_op jit(solution)/shard_map/all_to_all | solution.py:184
  134.3 0.0 copy-start.3
  134.3 0.9 shard_map.173
  135.2 5.7 %all-to-all-start.3 = ((bf16[32,24,128]{2,1,0:T(8,128)(2,1)}), bf16[32,24,128]{2,1,0:T(8,128)(2,1)S(1)}, u32[]{:S(2)}, u32[]{:S(2)}) async-start(bf16[32,24,128]{2,1,0:T(8,128)(2,1)} %bitcast.9), calls=%async_computation.3 | async-start | bytes 393216 | tf_op jit(solution)/shard_map/all_to_all | solution.py:184
  140.9 0.0 copy-done.3
  140.9 0.0 copy-done.4
  140.9 0.0 copy-done.5
  140.9 1.2 shard_map.172
  142.1 17.5 %all-to-all-done.3 = bf16[32,24,128]{2,1,0:T(8,128)(2,1)S(1)} async-done(((bf16[32,24,128]{2,1,0:T(8,128)(2,1)}), bf16[32,24,128]{2,1,0:T(8,128)(2,1)S(1)}, u32[]{:S(2)}, u32[]{:S(2)}) %all-to-all-start.3) | async-done | bytes 196640 | tf_op jit(solution)/shard_map/all_to_all | solution.py:184
  159.6 1.2 shard_map.174
  (2 shorter events, 0.0 us)
Async XLA Ops:
  39.2 6.9 %copy-start = (bf16[1,2048,256]{2,1,0:T(8,128)(2,1)S(1)}, bf16[1,2048,256]{2,1,0:T(8,128)(2,1)}, u32[]{:S(2)}) copy-start(bf16[1,2048,256]{2,1,0:T(8,128)(2,1)} %refs_1_.1) | copy-start | bytes 3145732
  39.2 27.8 %all-to-all-start.1 = ((bf16[16,384,128]{2,1,0:T(8,128)(2,1)}), bf16[16,384,128]{2,1,0:T(8,128)(2,1)S(1)}, u32[]{:S(2)}, u32[]{:S(2)}) async-start(bf16[16,384,128]{2,1,0:T(8,128)(2,1)} %shard_map.168), calls=%async_computation.1 | async-start | bytes 3145728 | tf_op jit(solution)/shard_map/all_to_all | solution.py:184
  46.1 31.9 %collective-permute-start = (bf16[1,2048,256]{2,1,0:T(8,128)(2,1)S(1)}, bf16[1,2048,256]{2,1,0:T(8,128)(2,1)}, u32[]{:S(2)}, u32[]{:S(2)}) collective-permute-start(bf16[1,2048,256]{2,1,0:T(8,128)(2,1)S(1)} %copy-done), channel_id=1, source_target_pairs={{0,1},{1,0},{2,3},{3,2},{4,5},{5,4},{6,7},{7,6},{8,9},{9,8},{10,11... | collective-permute-start | bytes 3145736 | tf_op jit(solution)/shard_map/ppermute | solution.py:259
  50.6 38.7 %collective-permute-start.1 = (bf16[1,2048,256]{2,1,0:T(8,128)(2,1)}, bf16[1,2048,256]{2,1,0:T(8,128)(2,1)}, u32[]{:S(2)}, u32[]{:S(2)}) collective-permute-start(bf16[1,2048,256]{2,1,0:T(8,128)(2,1)} %refs_2_.1), channel_id=1, source_target_pairs={{0,1},{1,0},{2,3},{3,2},{4,5},{5,4},{6,7},{7,6},{8,9},{9,8},{10,11... | collective-permute-start | bytes 3145736 | tf_op jit(solution)/shard_map/ppermute | solution.py:259
  52.6 47.9 %collective-permute-start.2 = (bf16[1,256,2048]{2,1,0:T(8,128)(2,1)}, bf16[1,256,2048]{2,1,0:T(8,128)(2,1)}, u32[]{:S(2)}, u32[]{:S(2)}) collective-permute-start(bf16[1,256,2048]{2,1,0:T(8,128)(2,1)} %refs_3_.5), channel_id=1, source_target_pairs={{0,1},{1,0},{2,3},{3,2},{4,5},{5,4},{6,7},{7,6},{8,9},{9,8},{10,11... | collective-permute-start | bytes 3145736 | tf_op jit(solution)/shard_map/ppermute | solution.py:259
  59.3 11.6 %collective-permute-start.3 = (bf16[32,128]{1,0:T(8,128)(2,1)S(1)}, bf16[32,128]{1,0:T(8,128)(2,1)S(1)}, u32[]{:S(2)}, u32[]{:S(2)}) collective-permute-start(bf16[32,128]{1,0:T(8,128)(2,1)S(1)} %get-tuple-element.7.refs_6_), channel_id=1, source_target_pairs={{0,16},{16,32},{32,48},{48,64},{64,80},{80,96},{96,112},{112,128},... | collective-permute-start | bytes 24584 | tf_op jit(solution)/shard_map/ppermute | solution.py:256
  67.0 1.2 copy-start.1
  68.2 1.2 copy-start.2
  134.3 6.6 %copy-start.3 = (bf16[512,128]{1,0:T(8,128)(2,1)S(1)}, bf16[512,128]{1,0:T(8,128)(2,1)}, u32[]{:S(2)}) copy-start(bf16[512,128]{1,0:T(8,128)(2,1)} %refs_3_.7) | copy-start | bytes 393220
  134.3 6.6 %copy-start.4 = (f32[512]{0:T(512)S(1)}, f32[512]{0:T(512)}, u32[]{:S(2)}) copy-start(f32[512]{0:T(512)} %param.22) | copy-start | bytes 6148
  134.3 6.6 %copy-start.5 = (f32[512]{0:T(512)S(1)}, f32[512]{0:T(512)}, u32[]{:S(2)}) copy-start(f32[512]{0:T(512)} %param.23) | copy-start | bytes 6148
  135.2 24.5 %all-to-all-start.3 = ((bf16[32,24,128]{2,1,0:T(8,128)(2,1)}), bf16[32,24,128]{2,1,0:T(8,128)(2,1)S(1)}, u32[]{:S(2)}, u32[]{:S(2)}) async-start(bf16[32,24,128]{2,1,0:T(8,128)(2,1)} %bitcast.9), calls=%async_computation.3 | async-start | bytes 393216 | tf_op jit(solution)/shard_map/all_to_all | solution.py:184

commit v6 on v5

--- a/solution.py
+++ b/solution.py
@@ -155,22 +155,37 @@
     out_ref[...] = lax.dot_general(activated, wo_ref[...], (((0,), (0,)), ((), ())), preferred_element_type=F32).astype(BF16)
 
 
-def add_parts(side, parts_ref, out_ref):
-    count, half = parts_ref.shape[0], out_ref.shape[0] // 2
+def add_parts(side, capacity, parts_ref, keep_ref, give_ref):
+    count, half = parts_ref.shape[0], keep_ref.shape[0]
+    core = lax.axis_index("ep") % 2
+    block = 2 * capacity
     for p in range(2):
         total = None
         for j in range(count):
             if row_class(j, side) == p:
                 term = parts_ref[j, :half, :].astype(F32)
                 total = term if total is None else total + term
-        out_ref[p * half : (p + 1) * half, :] = total.astype(BF16)
-
-
-def combine(back_ref, table_ref, out_ref):
-    rows_b = out_ref.shape[0]
+        total = total.astype(BF16)
+        for z in range(half // block):
+            even = total[z * block : z * block + capacity]
+            odd = total[z * block + capacity : (z + 1) * block]
+            at = (p * (half // block) + z) * capacity
+            keep_ref[at : at + capacity, :] = jnp.where(core == 0, even, odd)
+            give_ref[at : at + capacity, :] = jnp.where(core == 0, odd, even)
+
+
+def by_chip(capacity, keep_ref, came_ref, out_ref):
+    for z in range(out_ref.shape[0]):
+        out_ref[z, :capacity, :] = keep_ref[z * capacity : (z + 1) * capacity, :]
+        out_ref[z, capacity:, :] = came_ref[z * capacity : (z + 1) * capacity, :]
+
+
+def combine(capacity, back_ref, table_ref, out_ref):
     slots = back_ref.shape[0]
     table = jnp.transpose(table_ref[...])
-    place = lax.broadcasted_iota(jnp.int32, (rows_b, slots), 1).astype(F32)
+    place = lax.broadcasted_iota(jnp.int32, (1, slots), 1)
+    turn = jnp.where(place % (2 * capacity) < capacity, capacity, -capacity)
+    place = (place + turn * (lax.axis_index("ep") % 2)).astype(F32)
     back = back_ref[...]
     total = None
     for j in range(2):
@@ -180,8 +195,8 @@
     out_ref[...] = total.astype(BF16)
 
 
-def exchange(blocks, axis):
-    return lax.all_to_all(blocks, axis, split_axis=0, concat_axis=0, tiled=True)
+def exchange(blocks, axis, members=None):
+    return lax.all_to_all(blocks, axis, split_axis=0, concat_axis=0, tiled=True, axis_index_groups=members)
 
 
 def neighbours(groups, side, along_x):
@@ -269,15 +284,25 @@
     partials = exchange(partial, "tp")
 
     def total(*refs):
-        add_parts(side, *refs)
+        add_parts(side, capacity, *refs)
 
     def tail(*refs):
         mixer_tail(half, *refs)
 
-    (summed,) = call(total, [((slots, width), BF16)], partials)
+    def order(*refs):
+        by_chip(capacity, *refs)
+
+    def final(*refs):
+        combine(capacity, *refs)
+
+    keep, give = call(total, [((half, width), BF16)] * 2, partials)
+    came = lax.ppermute(give, "ep", [(e, e ^ 1) for e in range(groups)])
     (mixed,) = call(tail, [((tokens, width), BF16)], partials, channel_gain[None, :], channel_shift[None, :], mixer_out_weight)
-    returned = exchange(summed.reshape(groups, capacity, width), "ep").reshape(slots, width)
-    (combined,) = call(combine, [((rows_b, width), BF16)], returned, table)
+    chips = groups // 2
+    (outbound,) = call(order, [((chips, 2 * capacity, width), BF16)], keep, came)
+    same_core = [[2 * z + c for z in range(chips)] for c in range(2)]
+    returned = exchange(outbound, "ep", same_core).reshape(slots, width)
+    (combined,) = call(final, [((rows_b, width), BF16)], returned, table)
     return mixed, combined
 
 

time: 161 us -> 161 us (level); the launches traced: 161 us -> 157 us
  waiting for transfers between devices: 52.8 us -> 47.8 us
    all_to_all x2, waiting for transfers between devices: 23.2 us -> 17.3 us  [exchange(): lax.all_to_all(blocks, axis, split_axis=0, concat_axis=0, tiled=True, axi...]
    ppermute x0 -> x1, starting transfers between devices: none -> 2.79 us  [on_device(): came = lax.ppermute(give, 'ep', [(e, e ^ 1) for e in range(groups)])]
    pallas_call x8 -> x9, Pallas kernels: 13.5 us -> 13.5 us  [call(): pl.pallas_call(kernel, out_shape=tuple((jax.ShapeDtypeStruct(s, d) for s,...]
  transfers between devices with their start and end apart: 6 -> 7, of which waited for: 5 -> 6; matrix products, arithmetic and copies ran while one was open for 0% -> 0% of each run, Pallas kernels for 3% -> 3%
where the time goes in v6:
time: 161 us; the launch traced here: 157 us
  blocking collectives  65.7 us (41%)
  waiting for transfers between devices  47.8 us (30%)
  starting transfers between devices  27.2 us (17%)
  Pallas kernels  13.5 us (8%)
  local copies, waits for them, and re-layouts  2.46 us (2%)
    all_to_all x2, blocking collectives, exchange(): lax.all_to_all(blocks, axis, split_axis=0, concat_axis=0, tiled=True, axi...  65.7 us
    ppermute x3, waiting for transfers between devices, on_device(): lent.append(lax.ppermute(w, ('ep', 'tp'), neighbours(groups, side, True)))  29.6 us
    all_to_all x2, waiting for transfers between devices, exchange(): lax.all_to_all(blocks, axis, split_axis=0, concat_axis=0, tiled=True, axi...  17.3 us
    pallas_call x9, Pallas kernels, call(): pl.pallas_call(kernel, out_shape=tuple((jax.ShapeDtypeStruct(s, d) for s,...  13.5 us
    all_to_all x2, starting transfers between devices, exchange(): lax.all_to_all(blocks, axis, split_axis=0, concat_axis=0, tiled=True, axi...  11.4 us
    ppermute x3, starting transfers between devices, on_device(): lent.append(lax.ppermute(w, ('ep', 'tp'), neighbours(groups, side, True)))  11 us
  transfers between devices with their start and end apart: 7, of which 6 were waited for; matrix products, arithmetic and copies ran while one was open for 0% of the time, Pallas kernels for 3%

profile of v6, /device:TPU:1, one launch (start us, length us, event | category | flops | bytes accessed | tf_op | source)
XLA Modules:
  0.0 157.5 jit_solution(8680528573118637262)
XLA Ops:
  0.6 1.9 %shard_map.167 = (bf16[768,128]{1,0:T(8,128)(2,1)S(1)}, f32[8,256]{1,0:T(8,128)S(1)}) custom-call(s32[2,256]{1,0:T(2,128)} %bitcast.17, f32[2,256]{1,0:T(2,128)} %bitcast.18, f32[1,2048]{1,0:T(1,128)} %bitcast.15, bf16[256,2048]{1,0:T(8,128)(2,1)} %refs_3_.4), custom_call_target="tpu_custom_call" | custom-call | tf_op jit(solution)/shard_map/pallas_call | solution.py:40
  2.5 35.3 %all_to_all.20 = bf16[32,24,128]{2,1,0:T(8,128)(2,1)S(1)} all-to-all(bf16[32,24,128]{2,1,0:T(8,128)(2,1)S(1)} %bitcast.12), channel_id=1, replica_groups=mesh['ep'=32,'tp'=16] {'ep'}, dimensions={0} | all-to-all | bytes 393216 | tf_op jit(solution)/shard_map/all_to_all | solution.py:199
  37.8 1.4 shard_map.168
  39.2 0.0 copy-start
  39.2 6.9 %all-to-all-start.1 = ((bf16[16,384,128]{2,1,0:T(8,128)(2,1)}), bf16[16,384,128]{2,1,0:T(8,128)(2,1)S(1)}, u32[]{:S(2)}, u32[]{:S(2)}) async-start(bf16[16,384,128]{2,1,0:T(8,128)(2,1)} %shard_map.168), calls=%async_computation.1 | async-start | bytes 3145728 | tf_op jit(solution)/shard_map/all_to_all | solution.py:199
  46.1 0.0 copy-done
  46.1 4.5 %collective-permute-start = (bf16[1,2048,256]{2,1,0:T(8,128)(2,1)S(1)}, bf16[1,2048,256]{2,1,0:T(8,128)(2,1)}, u32[]{:S(2)}, u32[]{:S(2)}) collective-permute-start(bf16[1,2048,256]{2,1,0:T(8,128)(2,1)S(1)} %copy-done), channel_id=1, source_target_pairs={{0,1},{1,0},{2,3},{3,2},{4,5},{5,4},{6,7},{7,6},{8,9},{9,8},{10,11... | collective-permute-start | bytes 3145736 | tf_op jit(solution)/shard_map/ppermute | solution.py:274
  50.6 2.0 %collective-permute-start.1 = (bf16[1,2048,256]{2,1,0:T(8,128)(2,1)}, bf16[1,2048,256]{2,1,0:T(8,128)(2,1)}, u32[]{:S(2)}, u32[]{:S(2)}) collective-permute-start(bf16[1,2048,256]{2,1,0:T(8,128)(2,1)} %refs_2_.1), channel_id=1, source_target_pairs={{0,1},{1,0},{2,3},{3,2},{4,5},{5,4},{6,7},{7,6},{8,9},{9,8},{10,11... | collective-permute-start | bytes 3145736 | tf_op jit(solution)/shard_map/ppermute | solution.py:274
  52.6 4.5 %collective-permute-start.2 = (bf16[1,256,2048]{2,1,0:T(8,128)(2,1)}, bf16[1,256,2048]{2,1,0:T(8,128)(2,1)}, u32[]{:S(2)}, u32[]{:S(2)}) collective-permute-start(bf16[1,256,2048]{2,1,0:T(8,128)(2,1)} %refs_3_.5), channel_id=1, source_target_pairs={{0,1},{1,0},{2,3},{3,2},{4,5},{5,4},{6,7},{7,6},{8,9},{9,8},{10,11... | collective-permute-start | bytes 3145736 | tf_op jit(solution)/shard_map/ppermute | solution.py:274
  57.1 2.1 %shard_map.170 = (bf16[32,128]{1,0:T(8,128)(2,1)S(1)}, f32[32,32]{1,0:T(8,128)S(1)}) custom-call(f32[32,31]{1,0:T(8,128)} %refs_0_.1, f32[1,32]{1,0:T(1,128)} %bitcast.19, f32[1,2048]{1,0:T(1,128)} %bitcast.16, bf16[128,2048]{1,0:T(8,128)(2,1)} %refs_3_.6, bf16[32,2048]{1,0:T(8,128)(2,1)} %refs_4_.1, bf16[32,2048]{1,0:T(8,128)(2,1)} %refs_5_.1), custom_call_target="tpu_custom_call" | custom-call | tf_op jit(solution)/shard_map/pallas_call | solution.py:40
  59.3 2.0 %collective-permute-start.3 = (bf16[32,128]{1,0:T(8,128)(2,1)S(1)}, bf16[32,128]{1,0:T(8,128)(2,1)S(1)}, u32[]{:S(2)}, u32[]{:S(2)}) collective-permute-start(bf16[32,128]{1,0:T(8,128)(2,1)S(1)} %get-tuple-element.9.refs_6_), channel_id=1, source_target_pairs={{0,16},{16,32},{32,48},{48,64},{64,80},{80,96},{96,112},{112,128},... | collective-permute-start | bytes 24584 | tf_op jit(solution)/shard_map/ppermute | solution.py:271
  61.3 5.7 %all-to-all-done.1.refs_0_ = bf16[16,384,128]{2,1,0:T(8,128)(2,1)S(1)} async-done(((bf16[16,384,128]{2,1,0:T(8,128)(2,1)}), bf16[16,384,128]{2,1,0:T(8,128)(2,1)S(1)}, u32[]{:S(2)}, u32[]{:S(2)}) %all-to-all-start.1) | async-done | bytes 1572896 | tf_op jit(solution)/shard_map/all_to_all | solution.py:199
  67.0 1.2 copy-done.1
  68.2 1.2 copy-done.2
  69.4 1.4 shard_map.169.refs_1_
  70.9 0.0 collective-permute-done.3.refs_5_
  70.9 7.1 %collective-permute-done.refs_2_ = bf16[1,2048,256]{2,1,0:T(8,128)(2,1)} collective-permute-done((bf16[1,2048,256]{2,1,0:T(8,128)(2,1)S(1)}, bf16[1,2048,256]{2,1,0:T(8,128)(2,1)}, u32[]{:S(2)}, u32[]{:S(2)}) %collective-permute-start) | collective-permute-done | bytes 1048608 | tf_op jit(solution)/shard_map/ppermute | solution.py:274
  78.0 11.2 %collective-permute-done.1.refs_3_ = bf16[1,2048,256]{2,1,0:T(8,128)(2,1)} collective-permute-done((bf16[1,2048,256]{2,1,0:T(8,128)(2,1)}, bf16[1,2048,256]{2,1,0:T(8,128)(2,1)}, u32[]{:S(2)}, u32[]{:S(2)}) %collective-permute-start.1) | collective-permute-done | bytes 1048608 | tf_op jit(solution)/shard_map/ppermute | solution.py:274
  89.2 11.2 %collective-permute-done.2.refs_4_ = bf16[1,256,2048]{2,1,0:T(8,128)(2,1)} collective-permute-done((bf16[1,256,2048]{2,1,0:T(8,128)(2,1)}, bf16[1,256,2048]{2,1,0:T(8,128)(2,1)}, u32[]{:S(2)}, u32[]{:S(2)}) %collective-permute-start.2) | collective-permute-done | bytes 1048608 | tf_op jit(solution)/shard_map/ppermute | solution.py:274
  100.5 3.4 %shard_map.171 = bf16[16,416,128]{2,1,0:T(8,128)(2,1)S(1)} custom-call(bf16[16,384,128]{2,1,0:T(8,128)(2,1)S(1)} %all-to-all-done.1.refs_0_, f32[384,2048]{1,0:T(8,128)S(1)} %shard_map.169.refs_1_, bf16[1,2048,256]{2,1,0:T(8,128)(2,1)} %collective-permute-done.refs_2_, bf16[1,2048,256]{2,1,0:T(8,128)(2,1)} %collective-permute-done.1.refs_3_, ...), custom_call_target="tpu_custom_call" | custom-call | tf_op jit(solution)/shard_map/pallas_call | solution.py:40
  103.9 30.4 %all_to_all.21.refs_0_ = bf16[16,416,128]{2,1,0:T(8,128)(2,1)S(1)} all-to-all(bf16[16,416,128]{2,1,0:T(8,128)(2,1)S(1)} %shard_map.171), channel_id=1, replica_groups=mesh['ep'=32,'tp'=16] {'tp'}, dimensions={0} | all-to-all | bytes 3407872 | tf_op jit(solution)/shard_map/all_to_all | solution.py:199
  134.3 0.2 shard_map.173
  134.5 2.8 %collective-permute-start.4 = (bf16[384,128]{1,0:T(8,128)(2,1)S(1)}, bf16[384,128]{1,0:T(8,128)(2,1)S(1)}, u32[]{:S(2)}, u32[]{:S(2)}) collective-permute-start(bf16[384,128]{1,0:T(8,128)(2,1)S(1)} %get-tuple-element.12), channel_id=1, source_target_pairs={{0,16},{16,0},{32,48},{48,32},{64,80},{80,64},{96,112},{112,96},{1... | collective-permute-start | bytes 294920 | tf_op jit(solution)/shard_map/ppermute | solution.py:299
  137.3 0.9 collective-permute-done.4.refs_1_
  138.2 0.7 shard_map.174
  138.9 4.5 %all-to-all-start.3 = ((bf16[16,48,128]{2,1,0:T(8,128)(2,1)}), bf16[16,48,128]{2,1,0:T(8,128)(2,1)S(1)}, u32[]{:S(2)}, u32[]{:S(2)}) async-start(bf16[16,48,128]{2,1,0:T(8,128)(2,1)} %shard_map.174), calls=%async_computation.3 | async-start | bytes 393216 | tf_op jit(solution)/shard_map/all_to_all | solution.py:199
  143.4 0.0 copy-done.3
  143.4 0.0 copy-done.4
  143.4 0.0 copy-done.5
  143.4 1.2 shard_map.172
  144.7 11.6 %all-to-all-done.3 = bf16[16,48,128]{2,1,0:T(8,128)(2,1)S(1)} async-done(((bf16[16,48,128]{2,1,0:T(8,128)(2,1)}), bf16[16,48,128]{2,1,0:T(8,128)(2,1)S(1)}, u32[]{:S(2)}, u32[]{:S(2)}) %all-to-all-start.3) | async-done | bytes 196640 | tf_op jit(solution)/shard_map/all_to_all | solution.py:199
  156.3 1.2 shard_map.175
  (5 shorter events, 0.0 us)
Async XLA Ops:
  39.2 6.9 %copy-start = (bf16[1,2048,256]{2,1,0:T(8,128)(2,1)S(1)}, bf16[1,2048,256]{2,1,0:T(8,128)(2,1)}, u32[]{:S(2)}) copy-start(bf16[1,2048,256]{2,1,0:T(8,128)(2,1)} %refs_1_.1) | copy-start | bytes 3145732
  39.2 27.8 %all-to-all-start.1 = ((bf16[16,384,128]{2,1,0:T(8,128)(2,1)}), bf16[16,384,128]{2,1,0:T(8,128)(2,1)S(1)}, u32[]{:S(2)}, u32[]{:S(2)}) async-start(bf16[16,384,128]{2,1,0:T(8,128)(2,1)} %shard_map.168), calls=%async_computation.1 | async-start | bytes 3145728 | tf_op jit(solution)/shard_map/all_to_all | solution.py:199
  46.1 31.9 %collective-permute-start = (bf16[1,2048,256]{2,1,0:T(8,128)(2,1)S(1)}, bf16[1,2048,256]{2,1,0:T(8,128)(2,1)}, u32[]{:S(2)}, u32[]{:S(2)}) collective-permute-start(bf16[1,2048,256]{2,1,0:T(8,128)(2,1)S(1)} %copy-done), channel_id=1, source_target_pairs={{0,1},{1,0},{2,3},{3,2},{4,5},{5,4},{6,7},{7,6},{8,9},{9,8},{10,11... | collective-permute-start | bytes 3145736 | tf_op jit(solution)/shard_map/ppermute | solution.py:274
  50.6 38.7 %collective-permute-start.1 = (bf16[1,2048,256]{2,1,0:T(8,128)(2,1)}, bf16[1,2048,256]{2,1,0:T(8,128)(2,1)}, u32[]{:S(2)}, u32[]{:S(2)}) collective-permute-start(bf16[1,2048,256]{2,1,0:T(8,128)(2,1)} %refs_2_.1), channel_id=1, source_target_pairs={{0,1},{1,0},{2,3},{3,2},{4,5},{5,4},{6,7},{7,6},{8,9},{9,8},{10,11... | collective-permute-start | bytes 3145736 | tf_op jit(solution)/shard_map/ppermute | solution.py:274
  52.6 47.9 %collective-permute-start.2 = (bf16[1,256,2048]{2,1,0:T(8,128)(2,1)}, bf16[1,256,2048]{2,1,0:T(8,128)(2,1)}, u32[]{:S(2)}, u32[]{:S(2)}) collective-permute-start(bf16[1,256,2048]{2,1,0:T(8,128)(2,1)} %refs_3_.5), channel_id=1, source_target_pairs={{0,1},{1,0},{2,3},{3,2},{4,5},{5,4},{6,7},{7,6},{8,9},{9,8},{10,11... | collective-permute-start | bytes 3145736 | tf_op jit(solution)/shard_map/ppermute | solution.py:274
  59.3 11.6 %collective-permute-start.3 = (bf16[32,128]{1,0:T(8,128)(2,1)S(1)}, bf16[32,128]{1,0:T(8,128)(2,1)S(1)}, u32[]{:S(2)}, u32[]{:S(2)}) collective-permute-start(bf16[32,128]{1,0:T(8,128)(2,1)S(1)} %get-tuple-element.9.refs_6_), channel_id=1, source_target_pairs={{0,16},{16,32},{32,48},{48,64},{64,80},{80,96},{96,112},{112,128},... | collective-permute-start | bytes 24584 | tf_op jit(solution)/shard_map/ppermute | solution.py:271
  67.0 1.2 copy-start.1
  68.2 1.2 copy-start.2
  134.3 9.1 %copy-start.3 = (bf16[512,128]{1,0:T(8,128)(2,1)S(1)}, bf16[512,128]{1,0:T(8,128)(2,1)}, u32[]{:S(2)}) copy-start(bf16[512,128]{1,0:T(8,128)(2,1)} %refs_3_.7) | copy-start | bytes 393220
  134.3 9.1 %copy-start.4 = (f32[512]{0:T(512)S(1)}, f32[512]{0:T(512)}, u32[]{:S(2)}) copy-start(f32[512]{0:T(512)} %param.22) | copy-start | bytes 6148
  134.3 9.2 %copy-start.5 = (f32[512]{0:T(512)S(1)}, f32[512]{0:T(512)}, u32[]{:S(2)}) copy-start(f32[512]{0:T(512)} %param.23) | copy-start | bytes 6148
  134.5 3.7 %collective-permute-start.4 = (bf16[384,128]{1,0:T(8,128)(2,1)S(1)}, bf16[384,128]{1,0:T(8,128)(2,1)S(1)}, u32[]{:S(2)}, u32[]{:S(2)}) collective-permute-start(bf16[384,128]{1,0:T(8,128)(2,1)S(1)} %get-tuple-element.12), channel_id=1, source_target_pairs={{0,16},{16,0},{32,48},{48,32},{64,80},{80,64},{96,112},{112,96},{1... | collective-permute-start | bytes 294920 | tf_op jit(solution)/shard_map/ppermute | solution.py:299
  138.9 17.3 %all-to-all-start.3 = ((bf16[16,48,128]{2,1,0:T(8,128)(2,1)}), bf16[16,48,128]{2,1,0:T(8,128)(2,1)S(1)}, u32[]{:S(2)}, u32[]{:S(2)}) async-start(bf16[16,48,128]{2,1,0:T(8,128)(2,1)} %shard_map.174), calls=%async_computation.3 | async-start | bytes 393216 | tf_op jit(solution)/shard_map/all_to_all | solution.py:199

commit v7 on v6

--- a/solution.py
+++ b/solution.py
@@ -181,17 +181,15 @@
 
 
 def combine(capacity, back_ref, table_ref, out_ref):
+    rows_b = out_ref.shape[0]
     slots = back_ref.shape[0]
     table = jnp.transpose(table_ref[...])
     place = lax.broadcasted_iota(jnp.int32, (1, slots), 1)
     turn = jnp.where(place % (2 * capacity) < capacity, capacity, -capacity)
     place = (place + turn * (lax.axis_index("ep") % 2)).astype(F32)
-    back = back_ref[...]
-    total = None
-    for j in range(2):
-        pick = jnp.where(table[:, j : j + 1] == place, 1.0, 0.0).astype(BF16)
-        term = jnp.dot(pick, back, preferred_element_type=F32) * table[:, 2 + j : 3 + j]
-        total = term if total is None else total + term
+    picks = jnp.concatenate([jnp.where(table[:, j : j + 1] == place, 1.0, 0.0).astype(BF16) for j in range(2)], axis=0)
+    rows = jnp.dot(picks, back_ref[...], preferred_element_type=F32)
+    total = rows[:rows_b] * table[:, 2:3] + rows[rows_b:] * table[:, 3:4]
     out_ref[...] = total.astype(BF16)
 
 

time: 161 us -> 161 us (level)
  no operation moved by 1% of the time
where the time goes in v7:
time: 161 us; the launch traced here: 157 us
  blocking collectives  65.7 us (41%)
  waiting for transfers between devices  47.8 us (30%)
  starting transfers between devices  27.2 us (17%)
  Pallas kernels  13.5 us (8%)
  local copies, waits for them, and re-layouts  2.46 us (2%)
    all_to_all x2, blocking collectives, exchange(): lax.all_to_all(blocks, axis, split_axis=0, concat_axis=0, tiled=True, axi...  65.7 us
    ppermute x3, waiting for transfers between devices, on_device(): lent.append(lax.ppermute(w, ('ep', 'tp'), neighbours(groups, side, True)))  29.6 us
    all_to_all x2, waiting for transfers between devices, exchange(): lax.all_to_all(blocks, axis, split_axis=0, concat_axis=0, tiled=True, axi...  17.3 us
    pallas_call x9, Pallas kernels, call(): pl.pallas_call(kernel, out_shape=tuple((jax.ShapeDtypeStruct(s, d) for s,...  13.5 us
    all_to_all x2, starting transfers between devices, exchange(): lax.all_to_all(blocks, axis, split_axis=0, concat_axis=0, tiled=True, axi...  11.4 us
    ppermute x3, starting transfers between devices, on_device(): lent.append(lax.ppermute(w, ('ep', 'tp'), neighbours(groups, side, True)))  11 us
  transfers between devices with their start and end apart: 7, of which 6 were waited for; matrix products, arithmetic and copies ran while one was open for 0% of the time, Pallas kernels for 3%

profile of v7, /device:TPU:1, one launch (start us, length us, event | category | flops | bytes accessed | tf_op | source)
XLA Modules:
  0.0 157.5 jit_solution(8278665259760582510)
XLA Ops:
  0.6 1.9 %shard_map.167 = (bf16[768,128]{1,0:T(8,128)(2,1)S(1)}, f32[8,256]{1,0:T(8,128)S(1)}) custom-call(s32[2,256]{1,0:T(2,128)} %bitcast.17, f32[2,256]{1,0:T(2,128)} %bitcast.18, f32[1,2048]{1,0:T(1,128)} %bitcast.15, bf16[256,2048]{1,0:T(8,128)(2,1)} %refs_3_.4), custom_call_target="tpu_custom_call" | custom-call | tf_op jit(solution)/shard_map/pallas_call | solution.py:40
  2.5 35.3 %all_to_all.20 = bf16[32,24,128]{2,1,0:T(8,128)(2,1)S(1)} all-to-all(bf16[32,24,128]{2,1,0:T(8,128)(2,1)S(1)} %bitcast.12), channel_id=1, replica_groups=mesh['ep'=32,'tp'=16] {'ep'}, dimensions={0} | all-to-all | bytes 393216 | tf_op jit(solution)/shard_map/all_to_all | solution.py:197
  37.8 1.4 shard_map.168
  39.2 0.0 copy-start
  39.2 6.9 %all-to-all-start.1 = ((bf16[16,384,128]{2,1,0:T(8,128)(2,1)}), bf16[16,384,128]{2,1,0:T(8,128)(2,1)S(1)}, u32[]{:S(2)}, u32[]{:S(2)}) async-start(bf16[16,384,128]{2,1,0:T(8,128)(2,1)} %shard_map.168), calls=%async_computation.1 | async-start | bytes 3145728 | tf_op jit(solution)/shard_map/all_to_all | solution.py:197
  46.1 0.0 copy-done
  46.1 4.5 %collective-permute-start = (bf16[1,2048,256]{2,1,0:T(8,128)(2,1)S(1)}, bf16[1,2048,256]{2,1,0:T(8,128)(2,1)}, u32[]{:S(2)}, u32[]{:S(2)}) collective-permute-start(bf16[1,2048,256]{2,1,0:T(8,128)(2,1)S(1)} %copy-done), channel_id=1, source_target_pairs={{0,1},{1,0},{2,3},{3,2},{4,5},{5,4},{6,7},{7,6},{8,9},{9,8},{10,11... | collective-permute-start | bytes 3145736 | tf_op jit(solution)/shard_map/ppermute | solution.py:272
  50.6 2.0 %collective-permute-start.1 = (bf16[1,2048,256]{2,1,0:T(8,128)(2,1)}, bf16[1,2048,256]{2,1,0:T(8,128)(2,1)}, u32[]{:S(2)}, u32[]{:S(2)}) collective-permute-start(bf16[1,2048,256]{2,1,0:T(8,128)(2,1)} %refs_2_.1), channel_id=1, source_target_pairs={{0,1},{1,0},{2,3},{3,2},{4,5},{5,4},{6,7},{7,6},{8,9},{9,8},{10,11... | collective-permute-start | bytes 3145736 | tf_op jit(solution)/shard_map/ppermute | solution.py:272
  52.6 4.5 %collective-permute-start.2 = (bf16[1,256,2048]{2,1,0:T(8,128)(2,1)}, bf16[1,256,2048]{2,1,0:T(8,128)(2,1)}, u32[]{:S(2)}, u32[]{:S(2)}) collective-permute-start(bf16[1,256,2048]{2,1,0:T(8,128)(2,1)} %refs_3_.5), channel_id=1, source_target_pairs={{0,1},{1,0},{2,3},{3,2},{4,5},{5,4},{6,7},{7,6},{8,9},{9,8},{10,11... | collective-permute-start | bytes 3145736 | tf_op jit(solution)/shard_map/ppermute | solution.py:272
  57.1 2.1 %shard_map.170 = (bf16[32,128]{1,0:T(8,128)(2,1)S(1)}, f32[32,32]{1,0:T(8,128)S(1)}) custom-call(f32[32,31]{1,0:T(8,128)} %refs_0_.1, f32[1,32]{1,0:T(1,128)} %bitcast.19, f32[1,2048]{1,0:T(1,128)} %bitcast.16, bf16[128,2048]{1,0:T(8,128)(2,1)} %refs_3_.6, bf16[32,2048]{1,0:T(8,128)(2,1)} %refs_4_.1, bf16[32,2048]{1,0:T(8,128)(2,1)} %refs_5_.1), custom_call_target="tpu_custom_call" | custom-call | tf_op jit(solution)/shard_map/pallas_call | solution.py:40
  59.3 2.0 %collective-permute-start.3 = (bf16[32,128]{1,0:T(8,128)(2,1)S(1)}, bf16[32,128]{1,0:T(8,128)(2,1)S(1)}, u32[]{:S(2)}, u32[]{:S(2)}) collective-permute-start(bf16[32,128]{1,0:T(8,128)(2,1)S(1)} %get-tuple-element.9.refs_6_), channel_id=1, source_target_pairs={{0,16},{16,32},{32,48},{48,64},{64,80},{80,96},{96,112},{112,128},... | collective-permute-start | bytes 24584 | tf_op jit(solution)/shard_map/ppermute | solution.py:269
  61.3 5.7 %all-to-all-done.1.refs_0_ = bf16[16,384,128]{2,1,0:T(8,128)(2,1)S(1)} async-done(((bf16[16,384,128]{2,1,0:T(8,128)(2,1)}), bf16[16,384,128]{2,1,0:T(8,128)(2,1)S(1)}, u32[]{:S(2)}, u32[]{:S(2)}) %all-to-all-start.1) | async-done | bytes 1572896 | tf_op jit(solution)/shard_map/all_to_all | solution.py:197
  67.0 1.2 copy-done.1
  68.2 1.2 copy-done.2
  69.4 1.4 shard_map.169.refs_1_
  70.9 0.0 collective-permute-done.3.refs_5_
  70.9 7.1 %collective-permute-done.refs_2_ = bf16[1,2048,256]{2,1,0:T(8,128)(2,1)} collective-permute-done((bf16[1,2048,256]{2,1,0:T(8,128)(2,1)S(1)}, bf16[1,2048,256]{2,1,0:T(8,128)(2,1)}, u32[]{:S(2)}, u32[]{:S(2)}) %collective-permute-start) | collective-permute-done | bytes 1048608 | tf_op jit(solution)/shard_map/ppermute | solution.py:272
  78.0 11.2 %collective-permute-done.1.refs_3_ = bf16[1,2048,256]{2,1,0:T(8,128)(2,1)} collective-permute-done((bf16[1,2048,256]{2,1,0:T(8,128)(2,1)}, bf16[1,2048,256]{2,1,0:T(8,128)(2,1)}, u32[]{:S(2)}, u32[]{:S(2)}) %collective-permute-start.1) | collective-permute-done | bytes 1048608 | tf_op jit(solution)/shard_map/ppermute | solution.py:272
  89.2 11.2 %collective-permute-done.2.refs_4_ = bf16[1,256,2048]{2,1,0:T(8,128)(2,1)} collective-permute-done((bf16[1,256,2048]{2,1,0:T(8,128)(2,1)}, bf16[1,256,2048]{2,1,0:T(8,128)(2,1)}, u32[]{:S(2)}, u32[]{:S(2)}) %collective-permute-start.2) | collective-permute-done | bytes 1048608 | tf_op jit(solution)/shard_map/ppermute | solution.py:272
  100.5 3.4 %shard_map.171 = bf16[16,416,128]{2,1,0:T(8,128)(2,1)S(1)} custom-call(bf16[16,384,128]{2,1,0:T(8,128)(2,1)S(1)} %all-to-all-done.1.refs_0_, f32[384,2048]{1,0:T(8,128)S(1)} %shard_map.169.refs_1_, bf16[1,2048,256]{2,1,0:T(8,128)(2,1)} %collective-permute-done.refs_2_, bf16[1,2048,256]{2,1,0:T(8,128)(2,1)} %collective-permute-done.1.refs_3_, ...), custom_call_target="tpu_custom_call" | custom-call | tf_op jit(solution)/shard_map/pallas_call | solution.py:40
  103.9 30.4 %all_to_all.21.refs_0_ = bf16[16,416,128]{2,1,0:T(8,128)(2,1)S(1)} all-to-all(bf16[16,416,128]{2,1,0:T(8,128)(2,1)S(1)} %shard_map.171), channel_id=1, replica_groups=mesh['ep'=32,'tp'=16] {'tp'}, dimensions={0} | all-to-all | bytes 3407872 | tf_op jit(solution)/shard_map/all_to_all | solution.py:197
  134.3 0.2 shard_map.173
  134.5 2.8 %collective-permute-start.4 = (bf16[384,128]{1,0:T(8,128)(2,1)S(1)}, bf16[384,128]{1,0:T(8,128)(2,1)S(1)}, u32[]{:S(2)}, u32[]{:S(2)}) collective-permute-start(bf16[384,128]{1,0:T(8,128)(2,1)S(1)} %get-tuple-element.12), channel_id=1, source_target_pairs={{0,16},{16,0},{32,48},{48,32},{64,80},{80,64},{96,112},{112,96},{1... | collective-permute-start | bytes 294920 | tf_op jit(solution)/shard_map/ppermute | solution.py:297
  137.3 0.9 collective-permute-done.4.refs_1_
  138.2 0.7 shard_map.174
  138.9 4.5 %all-to-all-start.3 = ((bf16[16,48,128]{2,1,0:T(8,128)(2,1)}), bf16[16,48,128]{2,1,0:T(8,128)(2,1)S(1)}, u32[]{:S(2)}, u32[]{:S(2)}) async-start(bf16[16,48,128]{2,1,0:T(8,128)(2,1)} %shard_map.174), calls=%async_computation.3 | async-start | bytes 393216 | tf_op jit(solution)/shard_map/all_to_all | solution.py:197
  143.4 0.0 copy-done.3
  143.4 0.0 copy-done.4
  143.4 0.0 copy-done.5
  143.4 1.2 shard_map.172
  144.7 11.6 %all-to-all-done.3 = bf16[16,48,128]{2,1,0:T(8,128)(2,1)S(1)} async-done(((bf16[16,48,128]{2,1,0:T(8,128)(2,1)}), bf16[16,48,128]{2,1,0:T(8,128)(2,1)S(1)}, u32[]{:S(2)}, u32[]{:S(2)}) %all-to-all-start.3) | async-done | bytes 196640 | tf_op jit(solution)/shard_map/all_to_all | solution.py:197
  156.3 1.2 shard_map.175
  (5 shorter events, 0.0 us)
Async XLA Ops:
  39.2 6.9 %copy-start = (bf16[1,2048,256]{2,1,0:T(8,128)(2,1)S(1)}, bf16[1,2048,256]{2,1,0:T(8,128)(2,1)}, u32[]{:S(2)}) copy-start(bf16[1,2048,256]{2,1,0:T(8,128)(2,1)} %refs_1_.1) | copy-start | bytes 3145732
  39.2 27.8 %all-to-all-start.1 = ((bf16[16,384,128]{2,1,0:T(8,128)(2,1)}), bf16[16,384,128]{2,1,0:T(8,128)(2,1)S(1)}, u32[]{:S(2)}, u32[]{:S(2)}) async-start(bf16[16,384,128]{2,1,0:T(8,128)(2,1)} %shard_map.168), calls=%async_computation.1 | async-start | bytes 3145728 | tf_op jit(solution)/shard_map/all_to_all | solution.py:197
  46.1 31.9 %collective-permute-start = (bf16[1,2048,256]{2,1,0:T(8,128)(2,1)S(1)}, bf16[1,2048,256]{2,1,0:T(8,128)(2,1)}, u32[]{:S(2)}, u32[]{:S(2)}) collective-permute-start(bf16[1,2048,256]{2,1,0:T(8,128)(2,1)S(1)} %copy-done), channel_id=1, source_target_pairs={{0,1},{1,0},{2,3},{3,2},{4,5},{5,4},{6,7},{7,6},{8,9},{9,8},{10,11... | collective-permute-start | bytes 3145736 | tf_op jit(solution)/shard_map/ppermute | solution.py:272
  50.6 38.7 %collective-permute-start.1 = (bf16[1,2048,256]{2,1,0:T(8,128)(2,1)}, bf16[1,2048,256]{2,1,0:T(8,128)(2,1)}, u32[]{:S(2)}, u32[]{:S(2)}) collective-permute-start(bf16[1,2048,256]{2,1,0:T(8,128)(2,1)} %refs_2_.1), channel_id=1, source_target_pairs={{0,1},{1,0},{2,3},{3,2},{4,5},{5,4},{6,7},{7,6},{8,9},{9,8},{10,11... | collective-permute-start | bytes 3145736 | tf_op jit(solution)/shard_map/ppermute | solution.py:272
  52.6 47.9 %collective-permute-start.2 = (bf16[1,256,2048]{2,1,0:T(8,128)(2,1)}, bf16[1,256,2048]{2,1,0:T(8,128)(2,1)}, u32[]{:S(2)}, u32[]{:S(2)}) collective-permute-start(bf16[1,256,2048]{2,1,0:T(8,128)(2,1)} %refs_3_.5), channel_id=1, source_target_pairs={{0,1},{1,0},{2,3},{3,2},{4,5},{5,4},{6,7},{7,6},{8,9},{9,8},{10,11... | collective-permute-start | bytes 3145736 | tf_op jit(solution)/shard_map/ppermute | solution.py:272
  59.3 11.6 %collective-permute-start.3 = (bf16[32,128]{1,0:T(8,128)(2,1)S(1)}, bf16[32,128]{1,0:T(8,128)(2,1)S(1)}, u32[]{:S(2)}, u32[]{:S(2)}) collective-permute-start(bf16[32,128]{1,0:T(8,128)(2,1)S(1)} %get-tuple-element.9.refs_6_), channel_id=1, source_target_pairs={{0,16},{16,32},{32,48},{48,64},{64,80},{80,96},{96,112},{112,128},... | collective-permute-start | bytes 24584 | tf_op jit(solution)/shard_map/ppermute | solution.py:269
  67.0 1.2 copy-start.1
  68.2 1.2 copy-start.2
  134.3 9.1 %copy-start.3 = (bf16[512,128]{1,0:T(8,128)(2,1)S(1)}, bf16[512,128]{1,0:T(8,128)(2,1)}, u32[]{:S(2)}) copy-start(bf16[512,128]{1,0:T(8,128)(2,1)} %refs_3_.7) | copy-start | bytes 393220
  134.3 9.1 %copy-start.4 = (f32[512]{0:T(512)S(1)}, f32[512]{0:T(512)}, u32[]{:S(2)}) copy-start(f32[512]{0:T(512)} %param.22) | copy-start | bytes 6148
  134.3 9.2 %copy-start.5 = (f32[512]{0:T(512)S(1)}, f32[512]{0:T(512)}, u32[]{:S(2)}) copy-start(f32[512]{0:T(512)} %param.23) | copy-start | bytes 6148
  134.5 3.7 %collective-permute-start.4 = (bf16[384,128]{1,0:T(8,128)(2,1)S(1)}, bf16[384,128]{1,0:T(8,128)(2,1)S(1)}, u32[]{:S(2)}, u32[]{:S(2)}) collective-permute-start(bf16[384,128]{1,0:T(8,128)(2,1)S(1)} %get-tuple-element.12), channel_id=1, source_target_pairs={{0,16},{16,0},{32,48},{48,32},{64,80},{80,64},{96,112},{112,96},{1... | collective-permute-start | bytes 294920 | tf_op jit(solution)/shard_map/ppermute | solution.py:297
  138.9 17.3 %all-to-all-start.3 = ((bf16[16,48,128]{2,1,0:T(8,128)(2,1)}), bf16[16,48,128]{2,1,0:T(8,128)(2,1)S(1)}, u32[]{:S(2)}, u32[]{:S(2)}) async-start(bf16[16,48,128]{2,1,0:T(8,128)(2,1)} %shard_map.174), calls=%async_computation.3 | async-start | bytes 393216 | tf_op jit(solution)/shard_map/all_to_all | solution.py:197
